TPU v7x, 32 devices: a whole 2x2x4 slice. The times are simulated.
32 devices in a mesh: ep: 8 (over z, x), tp: 4 (over y, core).
Axes of the slice: x: 2, y: 2, z: 4, core: 2. Of those that a mesh axis runs over, the one named last changes fastest.
Arguments:
- out_gate: bfloat16 [8192, 1024], P('ep', 'tp'), may hold values from -6 to 6
- in_gate: bfloat16 [8192, 1024], P('ep', 'tp'), may hold values from -6 to 6
- conv_input: bfloat16 [8192, 1024], P('ep', 'tp'), may hold values from -6 to 6
- conv_taps: float32 [3, 1024], P(None, 'tp'), may hold values from -4 to 4
- group_gain: float32 [1024], P('tp'), may hold values from 0.1 to 1.9
- mix_out_w: bfloat16 [1024, 2048], replicated, may hold values from -0.1875 to 0.1875
- moe_in: bfloat16 [8192, 2048], P(('ep', 'tp')), may hold values from -6 to 6
- moe_gain: float32 [2048], replicated, may hold values from 0.1 to 1.9
- route_ids: int32 [8192, 2], P(('ep', 'tp')), may hold values from 0 to 31, as said below
- route_weight: float32 [8192, 2], P(('ep', 'tp')), may hold values from 0.1 to 1
- gate_w: bfloat16 [32, 2048, 1024], P(('ep', 'tp')), may hold values from -0.125 to 0.125
- up_w: bfloat16 [32, 2048, 1024], P(('ep', 'tp')), may hold values from -0.125 to 0.125
- down_w: bfloat16 [32, 1024, 2048], P(('ep', 'tp')), may hold values from -0.1875 to 0.1875
Outputs:
- mixed: bfloat16 [8192, 2048], P(('ep', 'tp'))
- moe_out: bfloat16 [8192, 2048], P(('ep', 'tp'))
Inputs may be any that keep to these rules, and one draw needn't show every extreme that they name: `route_ids`: the two numbers of a row are different experts of one group: group g holds experts g * 4 to g * 4 + 3. The rows of one device (aligned blocks of 256 rows) name each group in exactly 32 rows and each expert in exactly 16 rows.
All inputs are finite; a program needn't handle non-finite values.
Results may differ from a plain program's by a relative error of at most 0.0071.
Values may be sent and summed in bfloat16 or wider, within the bound.
No kernel may reach another device: no remote copies, remote signals or barrier semaphores. Data moves between devices by JAX's collectives and lax.ppermute only.
A program may use at most 128 MiB of HBM per device.

v0:
```python
import functools

import jax
import jax.numpy as jnp
from jax import lax
from jax.experimental import pallas as pl
from jax.experimental.pallas import tpu as pltpu
from jax.sharding import PartitionSpec as P


GROUP_CH = 64
LANES = 128
META = 16
EPS = 1e-06
F32 = jnp.float32
BF16 = jnp.bfloat16


VMEM = pl.BlockSpec(memory_space=pltpu.VMEM)
SMEM = pl.BlockSpec(memory_space=pltpu.SMEM)
HBM = pl.BlockSpec(memory_space=pltpu.HBM)


def dot(a, b):
    return jnp.dot(a, b, preferred_element_type=F32)


def dot_nt(a, b):
    return lax.dot_general(a, b, (((1,), (1,)), ((), ())), preferred_element_type=F32)


def iota(shape, dim):
    return lax.broadcasted_iota(jnp.int32, shape, dim)


def call(body, outs, specs, args, scratch, flops, vmem):
    return pl.pallas_call(
        body,
        out_shape=outs,
        in_specs=specs,
        out_specs=jax.tree.map(lambda _: VMEM, outs),
        scratch_shapes=scratch,
        cost_estimate=pl.CostEstimate(flops=flops, bytes_accessed=1 << 20, transcendentals=0),
        compiler_params=pltpu.CompilerParams(vmem_limit_bytes=vmem << 20),
    )(*args)


def swap(value, axis, mask):
    count = lax.axis_size(axis)
    return lax.ppermute(value, axis, [(i, i ^ mask) for i in range(count)])


def supers_of(n_chunks):
    return [part for part in (list(range(0, n_chunks, 2)), list(range(1, n_chunks, 2))) if part]


def fetch(pairs, sems):
    copies = [pltpu.make_async_copy(a, b, sems.at[n]) for n, (a, b) in enumerate(pairs)]
    for copy in copies:
        copy.start()
    return copies


def norm_rows(x_ref, gain, normed, width):
    tokens = x_ref.shape[0]
    step = min(64, tokens)

    def rows(r, carry):
        at = pl.ds(pl.multiple_of(r * step, step), step)
        wide = x_ref[at, :].astype(F32)
        scale = lax.rsqrt(jnp.mean(wide * wide, axis=-1, keepdims=True) + EPS)
        normed[at, :width] = (wide * scale * gain[...]).astype(BF16)
        return carry

    lax.fori_loop(0, tokens // step, rows, 0)


def ranks(sizes, ids, me):
    groups, members, per_group, _ = sizes
    tokens = ids.shape[1]
    experts = -(-groups * members // 16) * 16
    first, second = ids[0:1, :], ids[1:2, :]
    before = (iota((tokens, tokens), 0) < iota((tokens, tokens), 1)).astype(BF16)
    lane = iota((experts, tokens), 0)
    one, two = lane == first, lane == second
    seen = dot((one | two).astype(BF16), before)
    rank_one = jnp.sum(jnp.where(one, seen, 0.0), axis=0, keepdims=True)
    rank_two = jnp.sum(jnp.where(two, seen, 0.0), axis=0, keepdims=True)
    group = first // members
    rank = jnp.sum(jnp.where(lane // members == group, seen, 0.0), axis=0, keepdims=True) * 0.5
    mask = jnp.bitwise_xor(group, me)
    return rank_one, rank_two, (mask // 2) * (2 * per_group) + rank.astype(jnp.int32), jnp.bitwise_and(mask, 1)


def route_rows(sizes, ids, weights, normed, me):
    _, members, _, width = sizes
    tokens = normed.shape[0]
    first, second = ids[0:1, :], ids[1:2, :]
    rank_one, rank_two, base, odd = ranks(sizes, ids, me)
    parts = []
    for k in range(2):
        left = weights[k : k + 1, :]
        for _ in range(3):
            part = left.astype(BF16).astype(F32)
            parts.append(part)
            left = left - part
    row = iota((META, tokens), 0)
    meta = jnp.zeros((META, tokens), F32)
    fields = [(first % members).astype(F32), rank_one, (second % members).astype(F32), rank_two, *parts]
    for at, field in enumerate(fields):
        meta = jnp.where(row == at, field, meta)
    spread = (iota((LANES, META), 0) == iota((LANES, META), 1)).astype(BF16)
    flat = dot(spread, meta.astype(BF16)).astype(BF16)
    ident = (iota((tokens, tokens), 0) == iota((tokens, tokens), 1)).astype(BF16)
    normed[:, width:] = dot_nt(ident, flat).astype(BF16)
    return base, odd


def own_body(sizes, where, x, ids, weights, gain, normed, place):
    base, odd = route_rows(sizes, ids, weights, normed, where[0])
    place[...] = jnp.broadcast_to(jnp.where(odd == where[2], base, -1), place.shape)
    norm_rows(x, gain, normed, sizes[3])


def back_body(sizes, where, ids, pos):
    groups, _, per_group, _ = sizes
    _, _, base, odd = ranks(sizes, ids, where[0])
    back = jnp.where(odd == where[2], base, groups * per_group + base + per_group).astype(F32)
    pos[...] = jnp.broadcast_to(back, (pos.shape[1], pos.shape[0])).T


def prep_body(sizes, where, own, place_own, x_mate, ids_mate, weights_mate, gain, *refs):
    groups, _, per_group, width = sizes
    chunks, mate = refs[:-1], refs[-1]
    base, odd = route_rows(sizes, ids_mate, weights_mate, mate, where[0])
    norm_rows(x_mate, gain, mate, width)
    place_mate = jnp.where(odd == where[2], base + per_group, -1)
    total = groups * per_group
    tokens = mate.shape[0]
    picks = [(iota((total, tokens), 0) == place).astype(BF16) for place in (place_own[0:1, :], place_mate)]
    pick = jnp.concatenate(picks, axis=1)
    block = width // 4
    size = 2 * per_group

    def columns(n, carry):
        cols = pl.ds(pl.multiple_of(n * block, LANES), block)
        out = dot(pick, jnp.concatenate([own[:, cols], mate[:, cols]], axis=0)).astype(BF16)
        for k, ref in enumerate(chunks):
            ref[:, cols] = out[k * size : (k + 1) * size]
        return carry

    lax.fori_loop(0, 4, columns, 0)
    out = dot(pick, jnp.concatenate([own[:, width:], mate[:, width:]], axis=0)).astype(BF16)
    for k, ref in enumerate(chunks):
        ref[:, width:] = out[k * size : (k + 1) * size]


def expert_body(sizes, where, *refs):
    members, per_group, per_expert, width, count = sizes
    landed = [refs[m * count : (m + 1) * count] for m in range(members)]
    gate, up, down = refs[members * count : members * count + 3]
    outs, rows_x, hidden = refs[members * count + 3 : -2], refs[-2], refs[-1]
    me = where[1]
    size = 2 * per_group
    span = count * 2 * per_expert
    block = 512
    pick_row = (iota((META, LANES), 0) == iota((META, LANES), 1)).astype(BF16)
    for m in range(members):
        lanes = jnp.concatenate([r[:, width:] for r in landed[m]], axis=0)
        meta = dot_nt(pick_row, lanes).astype(jnp.int32)
        n = iota((1, count * size), 1)
        base = (n // size) * (2 * per_expert) + ((n % size) // per_group) * per_expert
        at = jnp.where(meta[0:1] == me, base + meta[1:2], jnp.where(meta[2:3] == me, base + meta[3:4], -1))
        pick = (iota((span, count * size), 0) == at).astype(BF16)
        for n in range(width // block):
            cols = slice(n * block, (n + 1) * block)
            value = jnp.concatenate([r[:, cols] for r in landed[m]], axis=0)
            rows_x[m * span : (m + 1) * span, cols] = dot(pick, value).astype(BF16)
    gated = dot(rows_x[...], gate[...])
    upper = dot(rows_x[...], up[...])
    hidden[...] = (gated / (1.0 + jnp.exp(-gated)) * upper).astype(BF16)
    out = dot(hidden[...], down[...]).astype(BF16)
    outs[0][...] = out[:span]
    outs[1][...] = out[span : 2 * span]
    for m in range(2, members, 2):
        outs[1 + m // 2][...] = out[m * span : (m + 2) * span]


def fetch_body(*refs):
    count = (len(refs) - 1) // 2
    for copy in fetch(list(zip(refs[:count], refs[count:-1])), refs[-1]):
        copy.wait()


def combine_body(sizes, where, *refs):
    _, per_group, per_expert, width, count = sizes
    metas, sources, outs = refs[:count], refs[count:-count], refs[-count:]
    me = where[1]
    size = 2 * per_group
    span = count * 2 * per_expert
    rows = count * size
    lanes = jnp.concatenate([r[:, width:] for r in metas], axis=0).astype(F32)
    n = iota((rows, 1), 0)
    base = (n // size) * (2 * per_expert) + ((n % size) // per_group) * per_expert
    depth = sum(r.shape[0] for r in sources)
    column = iota((rows, depth), 1)
    picks, weights = [], []
    for k in range(2):
        mask = jnp.bitwise_xor(lanes[:, 2 * k : 2 * k + 1].astype(jnp.int32), me)
        rank = lanes[:, 2 * k + 1 : 2 * k + 2].astype(jnp.int32)
        even = mask - jnp.bitwise_and(mask, 1)
        odd = jnp.bitwise_and(mask, 1)
        at = jnp.where(even == 0, odd * span, (2 * even - 2 + 3 * odd) * span)
        picks.append((column == at + base + rank).astype(BF16))
        w = 4 + 3 * k
        weights.append(lanes[:, w : w + 1] + lanes[:, w + 1 : w + 2] + lanes[:, w + 2 : w + 3])
    block = 512
    for c in range(width // block):
        cols = slice(c * block, (c + 1) * block)
        value = jnp.concatenate([r[:, cols] for r in sources], axis=0)
        out = (dot(picks[0], value) * weights[0] + dot(picks[1], value) * weights[1]).astype(BF16)
        for k, ref in enumerate(outs):
            ref[:, cols] = out[k * size : (k + 1) * size]


def final_body(pos, *refs):
    sources, out = refs[:-1], refs[-1]
    depth = sum(r.shape[0] for r in sources)
    tokens, width = out.shape
    pick = (iota((tokens, depth), 1) == pos[:, 0:1].astype(jnp.int32)).astype(BF16)
    block = 512
    for c in range(width // block):
        cols = slice(c * block, (c + 1) * block)
        value = jnp.concatenate([r[:, cols] for r in sources], axis=0)
        out[:, cols] = dot(pick, value).astype(BF16)


def conv_body(reach, where, edge, *refs):
    given, outs, taken = refs[:5], refs[5:-8], refs[-8:-3]
    product, normed, sems = refs[-3:]
    copies = fetch(list(zip(given, taken)), sems)
    in_gate, conv_input, out_gate, taps, gain = taken
    me = where[1]
    for copy in copies:
        copy.wait()
    rows, channels = in_gate.shape
    lead = edge.shape[0] // 2
    product[:lead] = edge[:lead].astype(F32) * edge[lead:].astype(F32)
    step = min(128, rows)
    share = (iota((channels, channels), 0) // GROUP_CH == iota((channels, channels), 1) // GROUP_CH).astype(F32) / GROUP_CH
    for r in range(rows // step):
        at = slice(r * step, (r + 1) * step)
        product[lead + r * step : lead + (r + 1) * step] = in_gate[at].astype(F32) * conv_input[at].astype(F32)
    for r in range(rows // step):
        at = slice(r * step, (r + 1) * step)
        total = None
        for tap in range(reach + 1):
            low = lead - reach + tap + r * step
            term = taps[tap : tap + 1, :] * product[low : low + step]
            total = term if total is None else total + term
        gated = out_gate[at].astype(F32) * total
        mean = jnp.dot(gated * gated, share, preferred_element_type=F32, precision=lax.Precision.HIGHEST)
        normed[at] = (gated * lax.rsqrt(mean + EPS) * gain[...]).astype(BF16)
    part = rows // len(outs)
    for m, ref in enumerate(outs):
        ref[...] = normed[pl.ds(pl.multiple_of(jnp.bitwise_xor(me, m) * part, part), part), :]


def mix_body(where, weight, *refs):
    blocks, out = refs[:-1], refs[-1]
    me = where[1]
    channels = blocks[0].shape[1]
    width = out.shape[1]
    block = 512

    def columns(n, carry):
        cols = pl.ds(pl.multiple_of(n * block, block), block)
        total = None
        for m, ref in enumerate(blocks):
            low = pl.multiple_of(jnp.bitwise_xor(me, m) * channels, channels)
            term = dot(ref[...], weight[pl.ds(low, channels), cols])
            total = term if total is None else total + term
        out[:, cols] = total.astype(BF16)
        return carry

    lax.fori_loop(0, width // block, columns, 0)


def shards(
    out_gate,
    in_gate,
    conv_input,
    conv_taps,
    group_gain,
    mix_out_w,
    moe_in,
    moe_gain,
    route_ids,
    route_weight,
    gate_w,
    up_w,
    down_w,
):
    members, groups = lax.axis_size("tp"), lax.axis_size("ep")
    me_ep, me_tp = lax.axis_index("ep"), lax.axis_index("tp")
    where = jnp.stack([me_ep, me_tp, me_tp % 2]).astype(jnp.int32)
    tokens, width = moe_in.shape
    inner = gate_w.shape[2]
    per_group = tokens // groups
    per_expert = 2 * per_group // members
    full = width + LANES
    size = 2 * per_group
    n_chunks = groups // 2

    rows, channels = in_gate.shape
    reach = conv_taps.shape[0] - 1

    x_mate = swap(moe_in, "tp", 1)
    ids, ids_mate = route_ids.T, swap(route_ids.T, "tp", 1)
    weights, weights_mate = route_weight.T, swap(route_weight.T, "tp", 1)
    gain = moe_gain.reshape(1, width)
    sizes_all = (groups, members, per_group, width)
    normed, place = call(
        functools.partial(own_body, sizes_all),
        [jax.ShapeDtypeStruct((tokens, full), BF16), jax.ShapeDtypeStruct((8, tokens), jnp.int32)],
        [SMEM] + [VMEM] * 4,
        (where, moe_in, ids, weights, gain),
        [],
        6 << 30,
        16,
    )
    leaving = call(
        functools.partial(prep_body, sizes_all),
        [jax.ShapeDtypeStruct((size, full), BF16)] * n_chunks,
        [SMEM] + [VMEM] * 6,
        (where, normed, place, x_mate, ids_mate, weights_mate, gain),
        [pltpu.VMEM((tokens, full), BF16)],
        20 << 30,
        16,
    )
    edge = jnp.concatenate([in_gate[rows - 8 :], conv_input[rows - 8 :]], axis=0)
    edge = lax.ppermute(edge, "ep", [(i, i + 1) for i in range(groups - 1)])

    def across(value, k):
        pairs = []
        for i in range(groups):
            for j in range(members):
                mask = 2 * k + j % 2
                if mask:
                    pairs.append((i * members + j, (i ^ mask) * members + j))
        got = lax.ppermute(value, ("ep", "tp"), pairs)
        return jnp.where(me_tp % 2 == 0, value, got) if k == 0 else got

    given = (gate_w[0], up_w[0], down_w[0])
    held = call(
        fetch_body,
        [jax.ShapeDtypeStruct(w.shape, BF16) for w in given],
        [HBM] * 3,
        given,
        [pltpu.SemaphoreType.DMA((3,))],
        1 << 30,
        2,
    )
    halves = supers_of(n_chunks)
    order = [k for half in halves for k in half]
    landed = {}
    for k in order:
        landed[k, 0] = across(leaving[k], k)
    for k in order:
        landed[k, 1] = swap(landed[k, 0], "tp", 1)
        for m in range(2, members, 2):
            landed[k, m] = swap(landed[k, 0], "tp", m)
            landed[k, m + 1] = swap(landed[k, m], "tp", 1)

    normed = call(
        functools.partial(conv_body, reach),
        [jax.ShapeDtypeStruct((rows // members, channels), BF16)] * members,
        [SMEM, VMEM] + [HBM] * 5,
        (where, edge, in_gate, conv_input, out_gate, conv_taps, group_gain.reshape(1, channels)),
        [pltpu.VMEM((rows, channels), BF16)] * 3
        + [
            pltpu.VMEM(conv_taps.shape, F32),
            pltpu.VMEM((1, channels), F32),
            pltpu.VMEM((rows + 8, channels), F32),
            pltpu.VMEM((rows, channels), BF16),
            pltpu.SemaphoreType.DMA((5,)),
        ],
        20 << 30,
        8,
    )
    blocks = [normed[0]] + [swap(normed[m], "tp", m) for m in range(1, members)]
    mixed = call(
        mix_body,
        jax.ShapeDtypeStruct((rows // members, width), BF16),
        [SMEM] + [VMEM] * (1 + members),
        (where, mix_out_w, *blocks),
        [],
        2 * (rows // members) * channels * members * width,
        8,
    )

    returned = {}
    for half in halves:
        count = len(half)
        span = count * 2 * per_expert
        sizes = (members, per_group, per_expert, width, count)
        outs = call(
            functools.partial(expert_body, sizes),
            [jax.ShapeDtypeStruct((span, width), BF16)] * 2
            + [jax.ShapeDtypeStruct((2 * span, width), BF16)] * (members // 2 - 1),
            [SMEM] + [VMEM] * (members * count + 3),
            (where, *[landed[k, m] for m in range(members) for k in half], *held),
            [pltpu.VMEM((members * span, width), BF16), pltpu.VMEM((members * span, inner), BF16)],
            6 * members * span * width * inner,
            16,
        )
        sources = [outs[0], swap(outs[1], "tp", 1)]
        for m in range(2, members, 2):
            there = swap(outs[1 + m // 2], "tp", m)
            sources += [there, swap(there, "tp", 1)]
        merged = call(
            functools.partial(combine_body, sizes),
            [jax.ShapeDtypeStruct((size, width), BF16)] * count,
            [SMEM] + [VMEM] * (count + len(sources)),
            (where, *[landed[k, 0] for k in half], *sources),
            [],
            4 * count * size * 6 * span * width,
            8,
        )
        for k, value in zip(half, merged):
            returned[k] = across(value, k)
    back_pos = call(
        functools.partial(back_body, sizes_all),
        jax.ShapeDtypeStruct((tokens, LANES), F32),
        [SMEM, VMEM],
        (where, ids),
        [],
        1 << 20,
        8,
    )
    ordered = [returned[k] for k in range(n_chunks)]
    moe_out = call(
        final_body,
        jax.ShapeDtypeStruct((tokens, width), BF16),
        [VMEM] * (1 + 2 * n_chunks),
        (back_pos, *ordered, *[swap(value, "tp", 1) for value in ordered]),
        [],
        4 * tokens * tokens * width,
        8,
    )
    return (mixed, moe_out)


def solution(mesh):
    in_specs = (
        P("ep", "tp"),
        P("ep", "tp"),
        P("ep", "tp"),
        P(None, "tp"),
        P("tp"),
        P(),
        P(("ep", "tp"), None),
        P(),
        P(("ep", "tp"), None),
        P(("ep", "tp"), None),
        P(("ep", "tp"), None, None),
        P(("ep", "tp"), None, None),
        P(("ep", "tp"), None, None),
    )
    out_specs = (P(("ep", "tp"), None), P(("ep", "tp"), None))

    return jax.shard_map(shards, mesh=mesh, in_specs=in_specs, out_specs=out_specs, check_vma=False)
```

profile of v0, /device:TPU:0, one launch (start us, length us, event | category | flops | bytes accessed | tf_op | source)
XLA Modules:
  0.0 136.9 jit_solution(14593305390217001813)
XLA Ops:
  6.8 3.2 %shard_map.144 = (bf16[64,2176]{1,0:T(8,128)(2,1)S(1)}, bf16[64,2176]{1,0:T(8,128)(2,1)S(1)}, bf16[64,2176]{1,0:T(8,128)(2,1)S(1)}, bf16[64,2176]{1,0:T(8,128)(2,1)S(1)}) custom-call(s32[3]{0:T(128)S(1)} %pad_add_fusion.where, bf16[256,2176]{1,0:T(8,128)(2,1)S(1)} %get-tuple-element.29.own, s32[8,256]{1,0:T(8,128)S(1)} %get-tuple-element.30.place_own, ...), custom_call_target="tpu_custom_call" | custom-call | flops 21474836480 | bytes 1048576 | tf_op jit(solution)/shard_map/pallas_call | solution.py:37
  10.0 2.7 %collective-permute-start.19 = (bf16[64,2176]{1,0:T(8,128)(2,1)S(1)}, bf16[64,2176]{1,0:T(8,128)(2,1)S(1)}, u32[]{:S(2)}, u32[]{:S(2)}) collective-permute-start(bf16[64,2176]{1,0:T(8,128)(2,1)S(1)} %get-tuple-element.40), channel_id=1, source_target_pairs={{0,8},{1,13},{2,10},{3,15},{4,12},{5,9},{6,14},{7,11},{8,0},{9,5},... | collective-permute-start | bytes 835592 | tf_op jit(solution)/shard_map/ppermute | solution.py:351
  13.4 2.5 %collective-permute-start.20 = (bf16[64,2176]{1,0:T(8,128)(2,1)S(1)}, bf16[64,2176]{1,0:T(8,128)(2,1)S(1)}, u32[]{:S(2)}, u32[]{:S(2)}) collective-permute-start(bf16[64,2176]{1,0:T(8,128)(2,1)S(1)} %get-tuple-element.41), channel_id=1, source_target_pairs={{0,24},{1,29},{2,26},{3,31},{4,28},{5,25},{6,30},{7,27},{8,16},{9,... | collective-permute-start | bytes 835592 | tf_op jit(solution)/shard_map/ppermute | solution.py:351
  16.1 3.3 %collective-permute-done.19.refs_0_ = bf16[64,2176]{1,0:T(8,128)(2,1)S(1)} collective-permute-done((bf16[64,2176]{1,0:T(8,128)(2,1)S(1)}, bf16[64,2176]{1,0:T(8,128)(2,1)S(1)}, u32[]{:S(2)}, u32[]{:S(2)}) %collective-permute-start.19) | collective-permute-done | bytes 278560 | tf_op jit(solution)/shard_map/ppermute | solution.py:351
  19.4 2.4 %collective-permute-start.23 = (bf16[64,2176]{1,0:T(8,128)(2,1)S(1)}, bf16[64,2176]{1,0:T(8,128)(2,1)S(1)}, u32[]{:S(2)}, u32[]{:S(2)}) collective-permute-start(bf16[64,2176]{1,0:T(8,128)(2,1)S(1)} %collective-permute-done.19.refs_0_), channel_id=1, source_target_pairs={{0,2},{1,3},{2,0},{3,1},{4,6},{5,7},{6,4},{7,5},{8,10},{9,11},{10,... | collective-permute-start | bytes 835592 | tf_op jit(solution)/shard_map/ppermute | solution.py:50
  21.9 17.6 %collective-permute-done.8.refs_1_ = bf16[64,2176]{1,0:T(8,128)(2,1)S(1)} collective-permute-done((bf16[64,2176]{1,0:T(8,128)(2,1)S(1)}, bf16[64,2176]{1,0:T(8,128)(2,1)S(1)}, u32[]{:S(2)}, u32[]{:S(2)}) %collective-permute-start.8) | collective-permute-done | bytes 278560 | tf_op jit(solution)/shard_map/ppermute | solution.py:351
  41.6 2.1 %collective-permute-start.9 = (bf16[64,2176]{1,0:T(8,128)(2,1)S(1)}, bf16[64,2176]{1,0:T(8,128)(2,1)S(1)}, u32[]{:S(2)}, u32[]{:S(2)}) collective-permute-start(bf16[64,2176]{1,0:T(8,128)(2,1)S(1)} %broadcast_select_fusion.refs_0_), channel_id=1, source_target_pairs={{0,1},{1,0},{2,3},{3,2},{4,5},{5,4},{6,7},{7,6},{8,9},{9,8},{10,11... | collective-permute-start | bytes 835592 | tf_op jit(solution)/shard_map/ppermute | solution.py:50
  44.2 3.3 %collective-permute-done.12.refs_5_ = bf16[64,2176]{1,0:T(8,128)(2,1)S(1)} collective-permute-done((bf16[64,2176]{1,0:T(8,128)(2,1)S(1)}, bf16[64,2176]{1,0:T(8,128)(2,1)S(1)}, u32[]{:S(2)}, u32[]{:S(2)}) %collective-permute-start.12) | collective-permute-done | bytes 278560 | tf_op jit(solution)/shard_map/ppermute | solution.py:50
  47.5 3.4 %collective-permute-start.14 = (bf16[64,2176]{1,0:T(8,128)(2,1)S(1)}, bf16[64,2176]{1,0:T(8,128)(2,1)S(1)}, u32[]{:S(2)}, u32[]{:S(2)}) collective-permute-start(bf16[64,2176]{1,0:T(8,128)(2,1)S(1)} %collective-permute-done.12.refs_5_), channel_id=1, source_target_pairs={{0,1},{1,0},{2,3},{3,2},{4,5},{5,4},{6,7},{7,6},{8,9},{9,8},{10,11... | collective-permute-start | bytes 835592 | tf_op jit(solution)/shard_map/ppermute | solution.py:50
  50.9 2.2 %copy-done = bf16[1,2048,1024]{2,1,0:T(8,128)(2,1)S(1)} copy-done((bf16[1,2048,1024]{2,1,0:T(8,128)(2,1)S(1)}, bf16[1,2048,1024]{2,1,0:T(8,128)(2,1)}, u32[]{:S(2)}) %copy-start) | copy-done | bytes 4194328
  53.1 2.2 %copy-done.1 = bf16[1,2048,1024]{2,1,0:T(8,128)(2,1)S(1)} copy-done((bf16[1,2048,1024]{2,1,0:T(8,128)(2,1)S(1)}, bf16[1,2048,1024]{2,1,0:T(8,128)(2,1)}, u32[]{:S(2)}) %copy-start.1) | copy-done | bytes 4194328
  55.3 2.2 %copy-done.2 = bf16[1,1024,2048]{2,1,0:T(8,128)(2,1)S(1)} copy-done((bf16[1,1024,2048]{2,1,0:T(8,128)(2,1)S(1)}, bf16[1,1024,2048]{2,1,0:T(8,128)(2,1)}, u32[]{:S(2)}) %copy-start.2) | copy-done | bytes 4194328
  59.4 4.9 %shard_map.146 = (bf16[64,2048]{1,0:T(8,128)(2,1)S(1)}, bf16[64,2048]{1,0:T(8,128)(2,1)S(1)}, bf16[128,2048]{1,0:T(8,128)(2,1)S(1)}) custom-call(s32[3]{0:T(128)S(1)} %pad_add_fusion.where, bf16[64,2176]{1,0:T(8,128)(2,1)S(1)} %broadcast_select_fusion.refs_0_, bf16[64,2176]{1,0:T(8,128)(2,1)S(1)} %collective-permute-done.8.refs_1_, ...), custom_call_target="tpu_custom_call" | custom-call | flops 3221225472 | bytes 1048576 | tf_op jit(solution)/shard_map/pallas_call | solution.py:37
  66.1 5.0 %shard_map.148 = (bf16[64,2048]{1,0:T(8,128)(2,1)S(1)}, bf16[64,2048]{1,0:T(8,128)(2,1)S(1)}, bf16[128,2048]{1,0:T(8,128)(2,1)S(1)}) custom-call(s32[3]{0:T(128)S(1)} %pad_add_fusion.where, bf16[64,2176]{1,0:T(8,128)(2,1)S(1)} %collective-permute-done.19.refs_0_, bf16[64,2176]{1,0:T(8,128)(2,1)S(1)} %collective-permute-done.20.refs_1_, ...), custom_call_target="tpu_custom_call" | custom-call | flops 3221225472 | bytes 1048576 | tf_op jit(solution)/shard_map/pallas_call | solution.py:37
  71.6 7.7 %collective-permute-done.16.refs_4_ = bf16[128,2048]{1,0:T(8,128)(2,1)S(1)} collective-permute-done((bf16[128,2048]{1,0:T(8,128)(2,1)S(1)}, bf16[128,2048]{1,0:T(8,128)(2,1)S(1)}, u32[]{:S(2)}, u32[]{:S(2)}) %collective-permute-start.16) | collective-permute-done | bytes 524320 | tf_op jit(solution)/shard_map/ppermute | solution.py:50
  79.8 2.5 %collective-permute-start = (bf16[16,256]{1,0:T(8,128)(2,1)S(1)}, bf16[16,256]{1,0:T(8,128)(2,1)S(1)}, u32[]{:S(2)}, u32[]{:S(2)}) collective-permute-start(bf16[16,256]{1,0:T(8,128)(2,1)S(1)} %pad_maximum_fusion), channel_id=1, source_target_pairs={{0,4},{4,8},{8,12},{12,16},{16,20},{20,24},{24,28},{1,5},{5,9},{9,... | collective-permute-start | bytes 24584 | tf_op jit(solution)/shard_map/ppermute | solution.py:342
  82.4 7.3 %collective-permute-done.28.refs_4_ = bf16[128,2048]{1,0:T(8,128)(2,1)S(1)} collective-permute-done((bf16[128,2048]{1,0:T(8,128)(2,1)S(1)}, bf16[128,2048]{1,0:T(8,128)(2,1)S(1)}, u32[]{:S(2)}, u32[]{:S(2)}) %collective-permute-start.28) | collective-permute-done | bytes 524320 | tf_op jit(solution)/shard_map/ppermute | solution.py:50
  92.0 2.4 %shard_map.140 = (bf16[256,256]{1,0:T(8,128)(2,1)S(1)}, bf16[256,256]{1,0:T(8,128)(2,1)S(1)}, bf16[256,256]{1,0:T(8,128)(2,1)S(1)}, bf16[256,256]{1,0:T(8,128)(2,1)S(1)}) custom-call(s32[3]{0:T(128)S(1)} %pad_add_fusion.where, bf16[16,256]{1,0:T(8,128)(2,1)S(1)} %collective-permute-done.edge, bf16[1024,256]{1,0:T(8,128)(2,1)S(1)} %copy-done.7, ...), custom_call_target="tpu_custom_call" | custom-call | flops 21474836480 | bytes 1048576 | tf_op jit(solution)/shard_map/pallas_call | solution.py:37
  99.9 2.6 %collective-permute-start.32 = (bf16[64,2048]{1,0:T(8,128)(2,1)S(1)}, bf16[64,2048]{1,0:T(8,128)(2,1)S(1)}, u32[]{:S(2)}, u32[]{:S(2)}) collective-permute-start(bf16[64,2048]{1,0:T(8,128)(2,1)S(1)} %get-tuple-element.47), channel_id=1, source_target_pairs={{0,24},{1,29},{2,26},{3,31},{4,28},{5,25},{6,30},{7,27},{8,16},{9,... | collective-permute-start | bytes 786440 | tf_op jit(solution)/shard_map/ppermute | solution.py:351
  103.9 5.2 %collective-permute-done.30.refs_1_ = bf16[64,2048]{1,0:T(8,128)(2,1)S(1)} collective-permute-done((bf16[64,2048]{1,0:T(8,128)(2,1)S(1)}, bf16[64,2048]{1,0:T(8,128)(2,1)S(1)}, u32[]{:S(2)}, u32[]{:S(2)}) %collective-permute-start.30) | collective-permute-done | bytes 262176 | tf_op jit(solution)/shard_map/ppermute | solution.py:351
  109.0 6.2 %collective-permute-done.32.refs_3_ = bf16[64,2048]{1,0:T(8,128)(2,1)S(1)} collective-permute-done((bf16[64,2048]{1,0:T(8,128)(2,1)S(1)}, bf16[64,2048]{1,0:T(8,128)(2,1)S(1)}, u32[]{:S(2)}, u32[]{:S(2)}) %collective-permute-start.32) | collective-permute-done | bytes 262176 | tf_op jit(solution)/shard_map/ppermute | solution.py:351
  115.3 11.4 %collective-permute-done.31.refs_2_ = bf16[64,2048]{1,0:T(8,128)(2,1)S(1)} collective-permute-done((bf16[64,2048]{1,0:T(8,128)(2,1)S(1)}, bf16[64,2048]{1,0:T(8,128)(2,1)S(1)}, u32[]{:S(2)}, u32[]{:S(2)}) %collective-permute-start.31) | collective-permute-done | bytes 262176 | tf_op jit(solution)/shard_map/ppermute | solution.py:351
  128.1 3.7 %collective-permute-done.3.refs_3_ = bf16[256,256]{1,0:T(8,128)(2,1)S(1)} collective-permute-done((bf16[256,256]{1,0:T(8,128)(2,1)S(1)}, bf16[256,256]{1,0:T(8,128)(2,1)S(1)}, u32[]{:S(2)}, u32[]{:S(2)}) %collective-permute-start.3) | collective-permute-done | bytes 131104 | tf_op jit(solution)/shard_map/ppermute | solution.py:50
  131.8 3.3 %shard_map.141 = bf16[256,2048]{1,0:T(8,128)(2,1)} custom-call(s32[3]{0:T(128)S(1)} %pad_add_fusion.where, bf16[1024,2048]{1,0:T(8,128)(2,1)S(1)} %copy-done.3, bf16[256,256]{1,0:T(8,128)(2,1)S(1)} %get-tuple-element.25.refs_0_, bf16[256,256]{1,0:T(8,128)(2,1)S(1)} %collective-permute-done.1.refs_1_, bf16[256,256]{1,0:T(8,128)(2,1)S(1)} %collective-permute-done.2.refs_2_, ...), custom_call_target="tpu_custom_call" | custom-call | flops 1073741824 | bytes 1048576 | tf_op jit(solution)/shard_map/pallas_call | solution.py:37
  (99 shorter events, 26.7 us)
Async XLA Ops:
  10.0 9.4 %collective-permute-start.19 = (bf16[64,2176]{1,0:T(8,128)(2,1)S(1)}, bf16[64,2176]{1,0:T(8,128)(2,1)S(1)}, u32[]{:S(2)}, u32[]{:S(2)}) collective-permute-start(bf16[64,2176]{1,0:T(8,128)(2,1)S(1)} %get-tuple-element.40), channel_id=1, source_target_pairs={{0,8},{1,13},{2,10},{3,15},{4,12},{5,9},{6,14},{7,11},{8,0},{9,5},... | collective-permute-start | bytes 835592 | tf_op jit(solution)/shard_map/ppermute | solution.py:351
  13.4 27.7 %collective-permute-start.20 = (bf16[64,2176]{1,0:T(8,128)(2,1)S(1)}, bf16[64,2176]{1,0:T(8,128)(2,1)S(1)}, u32[]{:S(2)}, u32[]{:S(2)}) collective-permute-start(bf16[64,2176]{1,0:T(8,128)(2,1)S(1)} %get-tuple-element.41), channel_id=1, source_target_pairs={{0,24},{1,29},{2,26},{3,31},{4,28},{5,25},{6,30},{7,27},{8,16},{9,... | collective-permute-start | bytes 835592 | tf_op jit(solution)/shard_map/ppermute | solution.py:351
  15.9 23.7 %collective-permute-start.8 = (bf16[64,2176]{1,0:T(8,128)(2,1)S(1)}, bf16[64,2176]{1,0:T(8,128)(2,1)S(1)}, u32[]{:S(2)}, u32[]{:S(2)}) collective-permute-start(bf16[64,2176]{1,0:T(8,128)(2,1)S(1)} %get-tuple-element.32), channel_id=1, source_target_pairs={{0,16},{1,21},{2,18},{3,23},{4,20},{5,17},{6,22},{7,19},{8,24},{9,... | collective-permute-start | bytes 835592 | tf_op jit(solution)/shard_map/ppermute | solution.py:351
  19.4 24.3 %collective-permute-start.23 = (bf16[64,2176]{1,0:T(8,128)(2,1)S(1)}, bf16[64,2176]{1,0:T(8,128)(2,1)S(1)}, u32[]{:S(2)}, u32[]{:S(2)}) collective-permute-start(bf16[64,2176]{1,0:T(8,128)(2,1)S(1)} %collective-permute-done.19.refs_0_), channel_id=1, source_target_pairs={{0,2},{1,3},{2,0},{3,1},{4,6},{5,7},{6,4},{7,5},{8,10},{9,11},{10,... | collective-permute-start | bytes 835592 | tf_op jit(solution)/shard_map/ppermute | solution.py:50
  21.9 21.8 %collective-permute-start.11 = (bf16[64,2176]{1,0:T(8,128)(2,1)S(1)}, bf16[64,2176]{1,0:T(8,128)(2,1)S(1)}, u32[]{:S(2)}, u32[]{:S(2)}) collective-permute-start(bf16[64,2176]{1,0:T(8,128)(2,1)S(1)} %broadcast_select_fusion.refs_0_), channel_id=1, source_target_pairs={{0,2},{1,3},{2,0},{3,1},{4,6},{5,7},{6,4},{7,5},{8,10},{9,11},{10,... | collective-permute-start | bytes 835592 | tf_op jit(solution)/shard_map/ppermute | solution.py:50
  41.1 17.2 %collective-permute-start.24 = (bf16[64,2176]{1,0:T(8,128)(2,1)S(1)}, bf16[64,2176]{1,0:T(8,128)(2,1)S(1)}, u32[]{:S(2)}, u32[]{:S(2)}) collective-permute-start(bf16[64,2176]{1,0:T(8,128)(2,1)S(1)} %collective-permute-done.20.refs_1_), channel_id=1, source_target_pairs={{0,2},{1,3},{2,0},{3,1},{4,6},{5,7},{6,4},{7,5},{8,10},{9,11},{10,... | collective-permute-start | bytes 835592 | tf_op jit(solution)/shard_map/ppermute | solution.py:50
  41.6 16.8 %collective-permute-start.9 = (bf16[64,2176]{1,0:T(8,128)(2,1)S(1)}, bf16[64,2176]{1,0:T(8,128)(2,1)S(1)}, u32[]{:S(2)}, u32[]{:S(2)}) collective-permute-start(bf16[64,2176]{1,0:T(8,128)(2,1)S(1)} %broadcast_select_fusion.refs_0_), channel_id=1, source_target_pairs={{0,1},{1,0},{2,3},{3,2},{4,5},{5,4},{6,7},{7,6},{8,9},{9,8},{10,11... | collective-permute-start | bytes 835592 | tf_op jit(solution)/shard_map/ppermute | solution.py:50
  43.7 15.2 %collective-permute-start.10 = (bf16[64,2176]{1,0:T(8,128)(2,1)S(1)}, bf16[64,2176]{1,0:T(8,128)(2,1)S(1)}, u32[]{:S(2)}, u32[]{:S(2)}) collective-permute-start(bf16[64,2176]{1,0:T(8,128)(2,1)S(1)} %collective-permute-done.8.refs_1_), channel_id=1, source_target_pairs={{0,1},{1,0},{2,3},{3,2},{4,5},{5,4},{6,7},{7,6},{8,9},{9,8},{10,11... | collective-permute-start | bytes 835592 | tf_op jit(solution)/shard_map/ppermute | solution.py:50
  43.7 15.3 %collective-permute-start.13 = (bf16[64,2176]{1,0:T(8,128)(2,1)S(1)}, bf16[64,2176]{1,0:T(8,128)(2,1)S(1)}, u32[]{:S(2)}, u32[]{:S(2)}) collective-permute-start(bf16[64,2176]{1,0:T(8,128)(2,1)S(1)} %collective-permute-done.11.refs_4_), channel_id=1, source_target_pairs={{0,1},{1,0},{2,3},{3,2},{4,5},{5,4},{6,7},{7,6},{8,9},{9,8},{10,11... | collective-permute-start | bytes 835592 | tf_op jit(solution)/shard_map/ppermute | solution.py:50
  47.5 12.0 %collective-permute-start.14 = (bf16[64,2176]{1,0:T(8,128)(2,1)S(1)}, bf16[64,2176]{1,0:T(8,128)(2,1)S(1)}, u32[]{:S(2)}, u32[]{:S(2)}) collective-permute-start(bf16[64,2176]{1,0:T(8,128)(2,1)S(1)} %collective-permute-done.12.refs_5_), channel_id=1, source_target_pairs={{0,1},{1,0},{2,3},{3,2},{4,5},{5,4},{6,7},{7,6},{8,9},{9,8},{10,11... | collective-permute-start | bytes 835592 | tf_op jit(solution)/shard_map/ppermute | solution.py:50
  64.4 14.9 %collective-permute-start.16 = (bf16[128,2048]{1,0:T(8,128)(2,1)S(1)}, bf16[128,2048]{1,0:T(8,128)(2,1)S(1)}, u32[]{:S(2)}, u32[]{:S(2)}) collective-permute-start(bf16[128,2048]{1,0:T(8,128)(2,1)S(1)} %get-tuple-element.38), channel_id=1, source_target_pairs={{0,2},{1,3},{2,0},{3,1},{4,6},{5,7},{6,4},{7,5},{8,10},{9,11},{10,... | collective-permute-start | bytes 1572872 | tf_op jit(solution)/shard_map/ppermute | solution.py:50
  71.0 18.6 %collective-permute-start.28 = (bf16[128,2048]{1,0:T(8,128)(2,1)S(1)}, bf16[128,2048]{1,0:T(8,128)(2,1)S(1)}, u32[]{:S(2)}, u32[]{:S(2)}) collective-permute-start(bf16[128,2048]{1,0:T(8,128)(2,1)S(1)} %get-tuple-element.44), channel_id=1, source_target_pairs={{0,2},{1,3},{2,0},{3,1},{4,6},{5,7},{6,4},{7,5},{8,10},{9,11},{10,... | collective-permute-start | bytes 1572872 | tf_op jit(solution)/shard_map/ppermute | solution.py:50
  79.3 10.4 %collective-permute-start.17 = (bf16[128,2048]{1,0:T(8,128)(2,1)S(1)}, bf16[128,2048]{1,0:T(8,128)(2,1)S(1)}, u32[]{:S(2)}, u32[]{:S(2)}) collective-permute-start(bf16[128,2048]{1,0:T(8,128)(2,1)S(1)} %collective-permute-done.16.refs_4_), channel_id=1, source_target_pairs={{0,1},{1,0},{2,3},{3,2},{4,5},{5,4},{6,7},{7,6},{8,9},{9,8},{10,11... | collective-permute-start | bytes 1572872 | tf_op jit(solution)/shard_map/ppermute | solution.py:50
  79.3 10.4 %collective-permute-start.15 = (bf16[64,2048]{1,0:T(8,128)(2,1)S(1)}, bf16[64,2048]{1,0:T(8,128)(2,1)S(1)}, u32[]{:S(2)}, u32[]{:S(2)}) collective-permute-start(bf16[64,2048]{1,0:T(8,128)(2,1)S(1)} %get-tuple-element.37), channel_id=1, source_target_pairs={{0,1},{1,0},{2,3},{3,2},{4,5},{5,4},{6,7},{7,6},{8,9},{9,8},{10,11... | collective-permute-start | bytes 786440 | tf_op jit(solution)/shard_map/ppermute | solution.py:50
  79.8 12.1 %collective-permute-start = (bf16[16,256]{1,0:T(8,128)(2,1)S(1)}, bf16[16,256]{1,0:T(8,128)(2,1)S(1)}, u32[]{:S(2)}, u32[]{:S(2)}) collective-permute-start(bf16[16,256]{1,0:T(8,128)(2,1)S(1)} %pad_maximum_fusion), channel_id=1, source_target_pairs={{0,4},{4,8},{8,12},{12,16},{16,20},{20,24},{24,28},{1,5},{5,9},{9,... | collective-permute-start | bytes 24584 | tf_op jit(solution)/shard_map/ppermute | solution.py:342
  82.3 15.7 %collective-permute-start.27 = (bf16[64,2048]{1,0:T(8,128)(2,1)S(1)}, bf16[64,2048]{1,0:T(8,128)(2,1)S(1)}, u32[]{:S(2)}, u32[]{:S(2)}) collective-permute-start(bf16[64,2048]{1,0:T(8,128)(2,1)S(1)} %get-tuple-element.43), channel_id=1, source_target_pairs={{0,1},{1,0},{2,3},{3,2},{4,5},{5,4},{6,7},{7,6},{8,9},{9,8},{10,11... | collective-permute-start | bytes 786440 | tf_op jit(solution)/shard_map/ppermute | solution.py:50
  91.1 11.4 %collective-permute-start.18 = (bf16[64,2048]{1,0:T(8,128)(2,1)S(1)}, bf16[64,2048]{1,0:T(8,128)(2,1)S(1)}, u32[]{:S(2)}, u32[]{:S(2)}) collective-permute-start(bf16[64,2048]{1,0:T(8,128)(2,1)S(1)} %get-tuple-element.39), channel_id=1, source_target_pairs={{1,5},{3,7},{5,1},{7,3},{9,13},{11,15},{13,9},{15,11},{17,21},{19,... | collective-permute-start | bytes 786440 | tf_op jit(solution)/shard_map/ppermute | solution.py:351
  96.5 30.2 %collective-permute-start.2 = (bf16[256,256]{1,0:T(8,128)(2,1)S(1)}, bf16[256,256]{1,0:T(8,128)(2,1)S(1)}, u32[]{:S(2)}, u32[]{:S(2)}) collective-permute-start(bf16[256,256]{1,0:T(8,128)(2,1)S(1)} %get-tuple-element.27), channel_id=1, source_target_pairs={{0,2},{1,3},{2,0},{3,1},{4,6},{5,7},{6,4},{7,5},{8,10},{9,11},{10,... | collective-permute-start | bytes 393224 | tf_op jit(solution)/shard_map/ppermute | solution.py:50
  99.4 9.6 %collective-permute-start.30 = (bf16[64,2048]{1,0:T(8,128)(2,1)S(1)}, bf16[64,2048]{1,0:T(8,128)(2,1)S(1)}, u32[]{:S(2)}, u32[]{:S(2)}) collective-permute-start(bf16[64,2048]{1,0:T(8,128)(2,1)S(1)} %get-tuple-element.45), channel_id=1, source_target_pairs={{0,8},{1,13},{2,10},{3,15},{4,12},{5,9},{6,14},{7,11},{8,0},{9,5},... | collective-permute-start | bytes 786440 | tf_op jit(solution)/shard_map/ppermute | solution.py:351
  99.9 15.4 %collective-permute-start.32 = (bf16[64,2048]{1,0:T(8,128)(2,1)S(1)}, bf16[64,2048]{1,0:T(8,128)(2,1)S(1)}, u32[]{:S(2)}, u32[]{:S(2)}) collective-permute-start(bf16[64,2048]{1,0:T(8,128)(2,1)S(1)} %get-tuple-element.47), channel_id=1, source_target_pairs={{0,24},{1,29},{2,26},{3,31},{4,28},{5,25},{6,30},{7,27},{8,16},{9,... | collective-permute-start | bytes 786440 | tf_op jit(solution)/shard_map/ppermute | solution.py:351
  102.5 24.2 %collective-permute-start.31 = (bf16[64,2048]{1,0:T(8,128)(2,1)S(1)}, bf16[64,2048]{1,0:T(8,128)(2,1)S(1)}, u32[]{:S(2)}, u32[]{:S(2)}) collective-permute-start(bf16[64,2048]{1,0:T(8,128)(2,1)S(1)} %get-tuple-element.46), channel_id=1, source_target_pairs={{0,16},{1,21},{2,18},{3,23},{4,20},{5,17},{6,22},{7,19},{8,24},{9,... | collective-permute-start | bytes 786440 | tf_op jit(solution)/shard_map/ppermute | solution.py:351
  103.0 32.1 %collective-permute-start.33 = (bf16[64,2048]{1,0:T(8,128)(2,1)S(1)}, bf16[64,2048]{1,0:T(8,128)(2,1)S(1)}, u32[]{:S(2)}, u32[]{:S(2)}) collective-permute-start(bf16[64,2048]{1,0:T(8,128)(2,1)S(1)} %broadcast_select_fusion.1.refs_0_), channel_id=1, source_target_pairs={{0,1},{1,0},{2,3},{3,2},{4,5},{5,4},{6,7},{7,6},{8,9},{9,8},{10,11... | collective-permute-start | bytes 786440 | tf_op jit(solution)/shard_map/ppermute | solution.py:50
  109.0 26.1 %collective-permute-start.34 = (bf16[64,2048]{1,0:T(8,128)(2,1)S(1)}, bf16[64,2048]{1,0:T(8,128)(2,1)S(1)}, u32[]{:S(2)}, u32[]{:S(2)}) collective-permute-start(bf16[64,2048]{1,0:T(8,128)(2,1)S(1)} %collective-permute-done.30.refs_1_), channel_id=1, source_target_pairs={{0,1},{1,0},{2,3},{3,2},{4,5},{5,4},{6,7},{7,6},{8,9},{9,8},{10,11... | collective-permute-start | bytes 786440 | tf_op jit(solution)/shard_map/ppermute | solution.py:50
  115.3 19.9 %collective-permute-start.36 = (bf16[64,2048]{1,0:T(8,128)(2,1)S(1)}, bf16[64,2048]{1,0:T(8,128)(2,1)S(1)}, u32[]{:S(2)}, u32[]{:S(2)}) collective-permute-start(bf16[64,2048]{1,0:T(8,128)(2,1)S(1)} %collective-permute-done.32.refs_3_), channel_id=1, source_target_pairs={{0,1},{1,0},{2,3},{3,2},{4,5},{5,4},{6,7},{7,6},{8,9},{9,8},{10,11... | collective-permute-start | bytes 786440 | tf_op jit(solution)/shard_map/ppermute | solution.py:50
  (30 other events, 349.7 us)
where the time goes:
time: 137 us
  waiting for transfers between devices  65.8 us (48%)
  starting transfers between devices  33.4 us (24%)
  Pallas kernels  26.6 us (19%)
  local copies, waits for them, and re-layouts  9.91 us (7%)
    ppermute x8, waiting for transfers between devices, across(): got = lax.ppermute(value, ('ep', 'tp'), pairs)  43.8 us
    pallas_call x11, Pallas kernels, call(): pl.pallas_call(body, out_shape=outs, in_specs=specs, out_specs=jax.tree.m...  26.6 us
    ppermute x28, waiting for transfers between devices, swap(): return lax.ppermute(value, axis, [(i, i ^ mask) for i in range(count)])  22.1 us
    ppermute x28, starting transfers between devices, swap(): return lax.ppermute(value, axis, [(i, i ^ mask) for i in range(count)])  20.4 us
    ppermute x8, starting transfers between devices, across(): got = lax.ppermute(value, ('ep', 'tp'), pairs)  10.5 us
    unnamed x30, local copies, waits for them, and re-layouts  9.89 us
  transfers between devices with their start and end apart: 37, of which 9 were waited for; matrix products, arithmetic and copies ran while one was open for 0% of the time, Pallas kernels for 16%

commit v1 on v0

--- a/solution.py
+++ b/solution.py
@@ -50,8 +50,10 @@
     return lax.ppermute(value, axis, [(i, i ^ mask) for i in range(count)])
 
 
-def supers_of(n_chunks):
-    return [part for part in (list(range(0, n_chunks, 2)), list(range(1, n_chunks, 2))) if part]
+def units_of(n_chunks):
+    units = 4 if n_chunks >= 4 else 1
+    each = n_chunks // units
+    return [list(range(u * each, (u + 1) * each)) for u in range(units)]
 
 
 def fetch(pairs, sems):
@@ -180,16 +182,8 @@
     upper = dot(rows_x[...], up[...])
     hidden[...] = (gated / (1.0 + jnp.exp(-gated)) * upper).astype(BF16)
     out = dot(hidden[...], down[...]).astype(BF16)
-    outs[0][...] = out[:span]
-    outs[1][...] = out[span : 2 * span]
-    for m in range(2, members, 2):
-        outs[1 + m // 2][...] = out[m * span : (m + 2) * span]
-
-
-def fetch_body(*refs):
-    count = (len(refs) - 1) // 2
-    for copy in fetch(list(zip(refs[:count], refs[count:-1])), refs[-1]):
-        copy.wait()
+    for m, ref in enumerate(outs):
+        ref[...] = out[m * span : (m + 1) * span]
 
 
 def combine_body(sizes, where, *refs):
@@ -208,10 +202,7 @@
     for k in range(2):
         mask = jnp.bitwise_xor(lanes[:, 2 * k : 2 * k + 1].astype(jnp.int32), me)
         rank = lanes[:, 2 * k + 1 : 2 * k + 2].astype(jnp.int32)
-        even = mask - jnp.bitwise_and(mask, 1)
-        odd = jnp.bitwise_and(mask, 1)
-        at = jnp.where(even == 0, odd * span, (2 * even - 2 + 3 * odd) * span)
-        picks.append((column == at + base + rank).astype(BF16))
+        picks.append((column == mask * span + base + rank).astype(BF16))
         w = 4 + 3 * k
         weights.append(lanes[:, w : w + 1] + lanes[:, w + 1 : w + 2] + lanes[:, w + 2 : w + 3])
     block = 512
@@ -351,18 +342,9 @@
         got = lax.ppermute(value, ("ep", "tp"), pairs)
         return jnp.where(me_tp % 2 == 0, value, got) if k == 0 else got
 
-    given = (gate_w[0], up_w[0], down_w[0])
-    held = call(
-        fetch_body,
-        [jax.ShapeDtypeStruct(w.shape, BF16) for w in given],
-        [HBM] * 3,
-        given,
-        [pltpu.SemaphoreType.DMA((3,))],
-        1 << 30,
-        2,
-    )
-    halves = supers_of(n_chunks)
-    order = [k for half in halves for k in half]
+    held = (gate_w[0], up_w[0], down_w[0])
+    units = units_of(n_chunks)
+    order = range(n_chunks)
     landed = {}
     for k in order:
         landed[k, 0] = across(leaving[k], k)
@@ -400,34 +382,30 @@
     )
 
     returned = {}
-    for half in halves:
-        count = len(half)
+    for chunks in units:
+        count = len(chunks)
+        sizes = (members, per_group, per_expert, width, count)
         span = count * 2 * per_expert
-        sizes = (members, per_group, per_expert, width, count)
         outs = call(
             functools.partial(expert_body, sizes),
-            [jax.ShapeDtypeStruct((span, width), BF16)] * 2
-            + [jax.ShapeDtypeStruct((2 * span, width), BF16)] * (members // 2 - 1),
+            [jax.ShapeDtypeStruct((span, width), BF16)] * members,
             [SMEM] + [VMEM] * (members * count + 3),
-            (where, *[landed[k, m] for m in range(members) for k in half], *held),
+            (where, *[landed[k, m] for m in range(members) for k in chunks], *held),
             [pltpu.VMEM((members * span, width), BF16), pltpu.VMEM((members * span, inner), BF16)],
             6 * members * span * width * inner,
             16,
         )
-        sources = [outs[0], swap(outs[1], "tp", 1)]
-        for m in range(2, members, 2):
-            there = swap(outs[1 + m // 2], "tp", m)
-            sources += [there, swap(there, "tp", 1)]
+        sources = [outs[0]] + [swap(outs[m], "tp", m) for m in range(1, members)]
         merged = call(
             functools.partial(combine_body, sizes),
             [jax.ShapeDtypeStruct((size, width), BF16)] * count,
-            [SMEM] + [VMEM] * (count + len(sources)),
-            (where, *[landed[k, 0] for k in half], *sources),
+            [SMEM] + [VMEM] * (count + members),
+            (where, *[landed[k, 0] for k in chunks], *sources),
             [],
-            4 * count * size * 6 * span * width,
+            4 * count * size * members * span * width,
             8,
         )
-        for k, value in zip(half, merged):
+        for k, value in zip(chunks, merged):
             returned[k] = across(value, k)
     back_pos = call(
         functools.partial(back_body, sizes_all),
@@ -435,7 +413,7 @@
         [SMEM, VMEM],
         (where, ids),
         [],
-        1 << 20,
+        20 << 30,
         8,
     )
     ordered = [returned[k] for k in range(n_chunks)]

time: 137 us -> 131 us (0.956)
  waiting for transfers between devices: 65.8 us -> 48.9 us
  starting transfers between devices: 33.4 us -> 40.7 us
  Pallas kernels: 26.6 us -> 29.6 us
    ppermute x28 -> x34, waiting for transfers between devices: 22.1 us -> 8.33 us  [swap(): return lax.ppermute(value, axis, [(i, i ^ mask) for i in range(count)])]
    ppermute x28 -> x34, starting transfers between devices: 20.4 us -> 25.9 us  [swap(): return lax.ppermute(value, axis, [(i, i ^ mask) for i in range(count)])]
    ppermute x8, waiting for transfers between devices: 43.8 us -> 40.6 us  [across(): got = lax.ppermute(value, ('ep', 'tp'), pairs)]
    pallas_call x11 -> x14, Pallas kernels: 26.6 us -> 29.6 us  [call(): pl.pallas_call(body, out_shape=outs, in_specs=specs, out_specs=jax.tree.m...]
    unnamed x30 -> x32, local copies, waits for them, and re-layouts: 9.89 us -> 9.88 us
  transfers between devices with their start and end apart: 37 -> 43, of which waited for: 9 -> 7; matrix products, arithmetic and copies ran while one was open for 0% -> 0% of each run, Pallas kernels for 16% -> 19%
where the time goes in v1:
time: 131 us; the launch traced here: 130 us
  waiting for transfers between devices  48.9 us (37%)
  starting transfers between devices  40.7 us (31%)
  Pallas kernels  29.6 us (23%)
  local copies, waits for them, and re-layouts  9.9 us (8%)
    ppermute x8, waiting for transfers between devices, across(): got = lax.ppermute(value, ('ep', 'tp'), pairs)  40.6 us
    pallas_call x14, Pallas kernels, call(): pl.pallas_call(body, out_shape=outs, in_specs=specs, out_specs=jax.tree.m...  29.6 us
    ppermute x34, starting transfers between devices, swap(): return lax.ppermute(value, axis, [(i, i ^ mask) for i in range(count)])  25.9 us
    ppermute x8, starting transfers between devices, across(): got = lax.ppermute(value, ('ep', 'tp'), pairs)  11.4 us
    unnamed x32, local copies, waits for them, and re-layouts  9.88 us
    ppermute x34, waiting for transfers between devices, swap(): return lax.ppermute(value, axis, [(i, i ^ mask) for i in range(count)])  8.33 us
    ppermute x1, starting transfers between devices, shards(): edge = lax.ppermute(edge, 'ep', [(i, i + 1) for i in range(groups - 1)])  3.4 us
  transfers between devices with their start and end apart: 43, of which 7 were waited for; matrix products, arithmetic and copies ran while one was open for 0% of the time, Pallas kernels for 19%

profile of v1, /device:TPU:0, one launch (start us, length us, event | category | flops | bytes accessed | tf_op | source)
XLA Modules:
  0.0 130.3 jit_solution(5286447155962037543)
XLA Ops:
  5.1 1.7 %shard_map.143 = (bf16[256,2176]{1,0:T(8,128)(2,1)S(1)}, s32[8,256]{1,0:T(8,128)S(1)}) custom-call(s32[3]{0:T(128)S(1)} %pad_add_fusion.where, bf16[256,2048]{1,0:T(8,128)(2,1)S(1)} %copy-done.7, s32[2,256]{1,0:T(2,128)S(1)} %bitcast.27, f32[2,256]{1,0:T(2,128)S(1)} %bitcast.25, f32[1,2048]{1,0:T(1,128)S(1)} %bitcast.22), custom_call_target="tpu_custom_call" | custom-call | flops 6442450944 | bytes 1048576 | tf_op jit(solution)/shard_map/pallas_call | solution.py:37
  6.8 3.2 %shard_map.144 = (bf16[64,2176]{1,0:T(8,128)(2,1)S(1)}, bf16[64,2176]{1,0:T(8,128)(2,1)S(1)}, bf16[64,2176]{1,0:T(8,128)(2,1)S(1)}, bf16[64,2176]{1,0:T(8,128)(2,1)S(1)}) custom-call(s32[3]{0:T(128)S(1)} %pad_add_fusion.where, bf16[256,2176]{1,0:T(8,128)(2,1)S(1)} %get-tuple-element.32.own, s32[8,256]{1,0:T(8,128)S(1)} %get-tuple-element.33.place_own, ...), custom_call_target="tpu_custom_call" | custom-call | flops 21474836480 | bytes 1048576 | tf_op jit(solution)/shard_map/pallas_call | solution.py:37
  10.0 4.7 %collective-permute-start.31 = (bf16[64,2176]{1,0:T(8,128)(2,1)S(1)}, bf16[64,2176]{1,0:T(8,128)(2,1)S(1)}, u32[]{:S(2)}, u32[]{:S(2)}) collective-permute-start(bf16[64,2176]{1,0:T(8,128)(2,1)S(1)} %get-tuple-element.49), channel_id=1, source_target_pairs={{0,24},{1,29},{2,26},{3,31},{4,28},{5,25},{6,30},{7,27},{8,16},{9,... | collective-permute-start | bytes 835592 | tf_op jit(solution)/shard_map/ppermute | solution.py:342
  16.1 5.8 %collective-permute-done.31.refs_0_ = bf16[64,2176]{1,0:T(8,128)(2,1)S(1)} collective-permute-done((bf16[64,2176]{1,0:T(8,128)(2,1)S(1)}, bf16[64,2176]{1,0:T(8,128)(2,1)S(1)}, u32[]{:S(2)}, u32[]{:S(2)}) %collective-permute-start.31) | collective-permute-done | bytes 278560 | tf_op jit(solution)/shard_map/ppermute | solution.py:342
  21.9 2.0 %collective-permute-start.33 = (bf16[64,2176]{1,0:T(8,128)(2,1)S(1)}, bf16[64,2176]{1,0:T(8,128)(2,1)S(1)}, u32[]{:S(2)}, u32[]{:S(2)}) collective-permute-start(bf16[64,2176]{1,0:T(8,128)(2,1)S(1)} %collective-permute-done.31.refs_0_), channel_id=1, source_target_pairs={{0,2},{1,3},{2,0},{3,1},{4,6},{5,7},{6,4},{7,5},{8,10},{9,11},{10,... | collective-permute-start | bytes 835592 | tf_op jit(solution)/shard_map/ppermute | solution.py:50
  24.3 14.9 %collective-permute-done.23.refs_0_ = bf16[64,2176]{1,0:T(8,128)(2,1)S(1)} collective-permute-done((bf16[64,2176]{1,0:T(8,128)(2,1)S(1)}, bf16[64,2176]{1,0:T(8,128)(2,1)S(1)}, u32[]{:S(2)}, u32[]{:S(2)}) %collective-permute-start.23) | collective-permute-done | bytes 278560 | tf_op jit(solution)/shard_map/ppermute | solution.py:342
  41.8 6.9 %collective-permute-done.25.refs_2_ = bf16[64,2176]{1,0:T(8,128)(2,1)S(1)} collective-permute-done((bf16[64,2176]{1,0:T(8,128)(2,1)S(1)}, bf16[64,2176]{1,0:T(8,128)(2,1)S(1)}, u32[]{:S(2)}, u32[]{:S(2)}) %collective-permute-start.25) | collective-permute-done | bytes 278560 | tf_op jit(solution)/shard_map/ppermute | solution.py:50
  49.3 2.2 %copy-done = bf16[1,2048,1024]{2,1,0:T(8,128)(2,1)S(1)} copy-done((bf16[1,2048,1024]{2,1,0:T(8,128)(2,1)S(1)}, bf16[1,2048,1024]{2,1,0:T(8,128)(2,1)}, u32[]{:S(2)}) %copy-start) | copy-done | bytes 4194328
  51.4 2.2 %copy-done.2 = bf16[1,2048,1024]{2,1,0:T(8,128)(2,1)S(1)} copy-done((bf16[1,2048,1024]{2,1,0:T(8,128)(2,1)S(1)}, bf16[1,2048,1024]{2,1,0:T(8,128)(2,1)}, u32[]{:S(2)}) %copy-start.2) | copy-done | bytes 4194328
  53.6 2.2 %copy-done.3 = bf16[1,1024,2048]{2,1,0:T(8,128)(2,1)S(1)} copy-done((bf16[1,1024,2048]{2,1,0:T(8,128)(2,1)S(1)}, bf16[1,1024,2048]{2,1,0:T(8,128)(2,1)}, u32[]{:S(2)}) %copy-start.3) | copy-done | bytes 4194328
  55.8 3.2 %shard_map.151 = (bf16[32,2048]{1,0:T(8,128)(2,1)S(1)}, bf16[32,2048]{1,0:T(8,128)(2,1)S(1)}, bf16[32,2048]{1,0:T(8,128)(2,1)S(1)}, bf16[32,2048]{1,0:T(8,128)(2,1)S(1)}) custom-call(s32[3]{0:T(128)S(1)} %pad_add_fusion.where, bf16[64,2176]{1,0:T(8,128)(2,1)S(1)} %collective-permute-done.31.refs_0_, bf16[64,2176]{1,0:T(8,128)(2,1)S(1)} %collective-permute-done.32.refs_1_, ...), custom_call_target="tpu_custom_call" | custom-call | flops 1610612736 | bytes 1048576 | tf_op jit(solution)/shard_map/pallas_call | solution.py:37
  59.0 3.4 %collective-permute-start = (bf16[16,256]{1,0:T(8,128)(2,1)S(1)}, bf16[16,256]{1,0:T(8,128)(2,1)S(1)}, u32[]{:S(2)}, u32[]{:S(2)}) collective-permute-start(bf16[16,256]{1,0:T(8,128)(2,1)S(1)} %pad_maximum_fusion), channel_id=1, source_target_pairs={{0,4},{4,8},{8,12},{12,16},{16,20},{20,24},{24,28},{1,5},{5,9},{9,... | collective-permute-start | bytes 24584 | tf_op jit(solution)/shard_map/ppermute | solution.py:333
  63.0 3.2 %shard_map.145 = (bf16[32,2048]{1,0:T(8,128)(2,1)S(1)}, bf16[32,2048]{1,0:T(8,128)(2,1)S(1)}, bf16[32,2048]{1,0:T(8,128)(2,1)S(1)}, bf16[32,2048]{1,0:T(8,128)(2,1)S(1)}) custom-call(s32[3]{0:T(128)S(1)} %pad_add_fusion.where, bf16[64,2176]{1,0:T(8,128)(2,1)S(1)} %broadcast_select_fusion.refs_0_, bf16[64,2176]{1,0:T(8,128)(2,1)S(1)} %collective-permute-done.8.refs_1_, ...), custom_call_target="tpu_custom_call" | custom-call | flops 1610612736 | bytes 1048576 | tf_op jit(solution)/shard_map/pallas_call | solution.py:37
  68.1 3.2 %shard_map.149 = (bf16[32,2048]{1,0:T(8,128)(2,1)S(1)}, bf16[32,2048]{1,0:T(8,128)(2,1)S(1)}, bf16[32,2048]{1,0:T(8,128)(2,1)S(1)}, bf16[32,2048]{1,0:T(8,128)(2,1)S(1)}) custom-call(s32[3]{0:T(128)S(1)} %pad_add_fusion.where, bf16[64,2176]{1,0:T(8,128)(2,1)S(1)} %collective-permute-done.23.refs_0_, bf16[64,2176]{1,0:T(8,128)(2,1)S(1)} %collective-permute-done.24.refs_1_, ...), custom_call_target="tpu_custom_call" | custom-call | flops 1610612736 | bytes 1048576 | tf_op jit(solution)/shard_map/pallas_call | solution.py:37
  76.1 3.2 %shard_map.147 = (bf16[32,2048]{1,0:T(8,128)(2,1)S(1)}, bf16[32,2048]{1,0:T(8,128)(2,1)S(1)}, bf16[32,2048]{1,0:T(8,128)(2,1)S(1)}, bf16[32,2048]{1,0:T(8,128)(2,1)S(1)}) custom-call(s32[3]{0:T(128)S(1)} %pad_add_fusion.where, bf16[64,2176]{1,0:T(8,128)(2,1)S(1)} %collective-permute-done.15.refs_0_, bf16[64,2176]{1,0:T(8,128)(2,1)S(1)} %collective-permute-done.16.refs_1_, ...), custom_call_target="tpu_custom_call" | custom-call | flops 1610612736 | bytes 1048576 | tf_op jit(solution)/shard_map/pallas_call | solution.py:37
  81.0 1.6 %collective-permute-start.20 = (bf16[32,2048]{1,0:T(8,128)(2,1)S(1)}, bf16[32,2048]{1,0:T(8,128)(2,1)S(1)}, u32[]{:S(2)}, u32[]{:S(2)}) collective-permute-start(bf16[32,2048]{1,0:T(8,128)(2,1)S(1)} %get-tuple-element.42), channel_id=1, source_target_pairs={{0,2},{1,3},{2,0},{3,1},{4,6},{5,7},{6,4},{7,5},{8,10},{9,11},{10,... | collective-permute-start | bytes 393224 | tf_op jit(solution)/shard_map/ppermute | solution.py:50
  84.5 2.4 %shard_map.140 = (bf16[256,256]{1,0:T(8,128)(2,1)S(1)}, bf16[256,256]{1,0:T(8,128)(2,1)S(1)}, bf16[256,256]{1,0:T(8,128)(2,1)S(1)}, bf16[256,256]{1,0:T(8,128)(2,1)S(1)}) custom-call(s32[3]{0:T(128)S(1)} %pad_add_fusion.where, bf16[16,256]{1,0:T(8,128)(2,1)S(1)} %collective-permute-done.edge, bf16[1024,256]{1,0:T(8,128)(2,1)S(1)} %copy-done.6, ...), custom_call_target="tpu_custom_call" | custom-call | flops 21474836480 | bytes 1048576 | tf_op jit(solution)/shard_map/pallas_call | solution.py:37
  87.9 7.3 %collective-permute-start.1 = (bf16[256,256]{1,0:T(8,128)(2,1)S(1)}, bf16[256,256]{1,0:T(8,128)(2,1)S(1)}, u32[]{:S(2)}, u32[]{:S(2)}) collective-permute-start(bf16[256,256]{1,0:T(8,128)(2,1)S(1)} %get-tuple-element.29), channel_id=1, source_target_pairs={{0,1},{1,0},{2,3},{3,2},{4,5},{5,4},{6,7},{7,6},{8,9},{9,8},{10,11... | collective-permute-start | bytes 393224 | tf_op jit(solution)/shard_map/ppermute | solution.py:50
  96.2 1.6 %collective-permute-start.2 = (bf16[256,256]{1,0:T(8,128)(2,1)S(1)}, bf16[256,256]{1,0:T(8,128)(2,1)S(1)}, u32[]{:S(2)}, u32[]{:S(2)}) collective-permute-start(bf16[256,256]{1,0:T(8,128)(2,1)S(1)} %get-tuple-element.30), channel_id=1, source_target_pairs={{0,2},{1,3},{2,0},{3,1},{4,6},{5,7},{6,4},{7,5},{8,10},{9,11},{10,... | collective-permute-start | bytes 393224 | tf_op jit(solution)/shard_map/ppermute | solution.py:50
  98.0 2.9 %collective-permute-start.30 = (bf16[64,2048]{1,0:T(8,128)(2,1)S(1)}, bf16[64,2048]{1,0:T(8,128)(2,1)S(1)}, u32[]{:S(2)}, u32[]{:S(2)}) collective-permute-start(bf16[64,2048]{1,0:T(8,128)(2,1)S(1)} %shard_map.150), channel_id=1, source_target_pairs={{0,16},{1,21},{2,18},{3,23},{4,20},{5,17},{6,22},{7,19},{8,24},{9,... | collective-permute-start | bytes 786440 | tf_op jit(solution)/shard_map/ppermute | solution.py:342
  104.0 4.8 %collective-permute-done.38.refs_3_ = bf16[64,2048]{1,0:T(8,128)(2,1)S(1)} collective-permute-done((bf16[64,2048]{1,0:T(8,128)(2,1)S(1)}, bf16[64,2048]{1,0:T(8,128)(2,1)S(1)}, u32[]{:S(2)}, u32[]{:S(2)}) %collective-permute-start.38) | collective-permute-done | bytes 262176 | tf_op jit(solution)/shard_map/ppermute | solution.py:342
  108.8 15.1 %collective-permute-done.30.refs_2_ = bf16[64,2048]{1,0:T(8,128)(2,1)S(1)} collective-permute-done((bf16[64,2048]{1,0:T(8,128)(2,1)S(1)}, bf16[64,2048]{1,0:T(8,128)(2,1)S(1)}, u32[]{:S(2)}, u32[]{:S(2)}) %collective-permute-start.30) | collective-permute-done | bytes 262176 | tf_op jit(solution)/shard_map/ppermute | solution.py:342
  125.2 3.3 %shard_map.141 = bf16[256,2048]{1,0:T(8,128)(2,1)} custom-call(s32[3]{0:T(128)S(1)} %pad_add_fusion.where, bf16[1024,2048]{1,0:T(8,128)(2,1)S(1)} %copy-done.4, bf16[256,256]{1,0:T(8,128)(2,1)S(1)} %get-tuple-element.28.refs_0_, bf16[256,256]{1,0:T(8,128)(2,1)S(1)} %collective-permute-done.1.refs_1_, bf16[256,256]{1,0:T(8,128)(2,1)S(1)} %collective-permute-done.2.refs_2_, ...), custom_call_target="tpu_custom_call" | custom-call | flops 1073741824 | bytes 1048576 | tf_op jit(solution)/shard_map/pallas_call | solution.py:37
  128.6 1.7 %shard_map.153 = bf16[256,2048]{1,0:T(8,128)(2,1)} custom-call(f32[256,128]{1,0:T(8,128)S(1)} %shard_map.142.pos, bf16[64,2048]{1,0:T(8,128)(2,1)S(1)} %broadcast_select_fusion.1.refs_0_, bf16[64,2048]{1,0:T(8,128)(2,1)S(1)} %collective-permute-done.22.refs_1_, bf16[64,2048]{1,0:T(8,128)(2,1)S(1)} %collective-permute-done.30.refs_2_, ...), custom_call_target="tpu_custom_call" | custom-call | flops 536870912 | bytes 1048576 | tf_op jit(solution)/shard_map/pallas_call | solution.py:37
  (116 shorter events, 26.8 us)
Async XLA Ops:
  10.0 11.8 %collective-permute-start.31 = (bf16[64,2176]{1,0:T(8,128)(2,1)S(1)}, bf16[64,2176]{1,0:T(8,128)(2,1)S(1)}, u32[]{:S(2)}, u32[]{:S(2)}) collective-permute-start(bf16[64,2176]{1,0:T(8,128)(2,1)S(1)} %get-tuple-element.49), channel_id=1, source_target_pairs={{0,24},{1,29},{2,26},{3,31},{4,28},{5,25},{6,30},{7,27},{8,16},{9,... | collective-permute-start | bytes 835592 | tf_op jit(solution)/shard_map/ppermute | solution.py:342
  15.4 23.8 %collective-permute-start.23 = (bf16[64,2176]{1,0:T(8,128)(2,1)S(1)}, bf16[64,2176]{1,0:T(8,128)(2,1)S(1)}, u32[]{:S(2)}, u32[]{:S(2)}) collective-permute-start(bf16[64,2176]{1,0:T(8,128)(2,1)S(1)} %get-tuple-element.44), channel_id=1, source_target_pairs={{0,16},{1,21},{2,18},{3,23},{4,20},{5,17},{6,22},{7,19},{8,24},{9,... | collective-permute-start | bytes 835592 | tf_op jit(solution)/shard_map/ppermute | solution.py:342
  15.5 25.2 %collective-permute-start.15 = (bf16[64,2176]{1,0:T(8,128)(2,1)S(1)}, bf16[64,2176]{1,0:T(8,128)(2,1)S(1)}, u32[]{:S(2)}, u32[]{:S(2)}) collective-permute-start(bf16[64,2176]{1,0:T(8,128)(2,1)S(1)} %get-tuple-element.39), channel_id=1, source_target_pairs={{0,8},{1,13},{2,10},{3,15},{4,12},{5,9},{6,14},{7,11},{8,0},{9,5},... | collective-permute-start | bytes 835592 | tf_op jit(solution)/shard_map/ppermute | solution.py:342
  21.9 18.9 %collective-permute-start.33 = (bf16[64,2176]{1,0:T(8,128)(2,1)S(1)}, bf16[64,2176]{1,0:T(8,128)(2,1)S(1)}, u32[]{:S(2)}, u32[]{:S(2)}) collective-permute-start(bf16[64,2176]{1,0:T(8,128)(2,1)S(1)} %collective-permute-done.31.refs_0_), channel_id=1, source_target_pairs={{0,2},{1,3},{2,0},{3,1},{4,6},{5,7},{6,4},{7,5},{8,10},{9,11},{10,... | collective-permute-start | bytes 835592 | tf_op jit(solution)/shard_map/ppermute | solution.py:50
  23.8 17.5 %collective-permute-start.32 = (bf16[64,2176]{1,0:T(8,128)(2,1)S(1)}, bf16[64,2176]{1,0:T(8,128)(2,1)S(1)}, u32[]{:S(2)}, u32[]{:S(2)}) collective-permute-start(bf16[64,2176]{1,0:T(8,128)(2,1)S(1)} %collective-permute-done.31.refs_0_), channel_id=1, source_target_pairs={{0,1},{1,0},{2,3},{3,2},{4,5},{5,4},{6,7},{7,6},{8,9},{9,8},{10,11... | collective-permute-start | bytes 835592 | tf_op jit(solution)/shard_map/ppermute | solution.py:50
  23.9 17.6 %collective-permute-start.9 = (bf16[64,2176]{1,0:T(8,128)(2,1)S(1)}, bf16[64,2176]{1,0:T(8,128)(2,1)S(1)}, u32[]{:S(2)}, u32[]{:S(2)}) collective-permute-start(bf16[64,2176]{1,0:T(8,128)(2,1)S(1)} %broadcast_select_fusion.refs_0_), channel_id=1, source_target_pairs={{0,2},{1,3},{2,0},{3,1},{4,6},{5,7},{6,4},{7,5},{8,10},{9,11},{10,... | collective-permute-start | bytes 835592 | tf_op jit(solution)/shard_map/ppermute | solution.py:50
  39.2 9.5 %collective-permute-start.25 = (bf16[64,2176]{1,0:T(8,128)(2,1)S(1)}, bf16[64,2176]{1,0:T(8,128)(2,1)S(1)}, u32[]{:S(2)}, u32[]{:S(2)}) collective-permute-start(bf16[64,2176]{1,0:T(8,128)(2,1)S(1)} %collective-permute-done.23.refs_0_), channel_id=1, source_target_pairs={{0,2},{1,3},{2,0},{3,1},{4,6},{5,7},{6,4},{7,5},{8,10},{9,11},{10,... | collective-permute-start | bytes 835592 | tf_op jit(solution)/shard_map/ppermute | solution.py:50
  40.7 18.3 %collective-permute-start.17 = (bf16[64,2176]{1,0:T(8,128)(2,1)S(1)}, bf16[64,2176]{1,0:T(8,128)(2,1)S(1)}, u32[]{:S(2)}, u32[]{:S(2)}) collective-permute-start(bf16[64,2176]{1,0:T(8,128)(2,1)S(1)} %collective-permute-done.15.refs_0_), channel_id=1, source_target_pairs={{0,2},{1,3},{2,0},{3,1},{4,6},{5,7},{6,4},{7,5},{8,10},{9,11},{10,... | collective-permute-start | bytes 835592 | tf_op jit(solution)/shard_map/ppermute | solution.py:50
  41.3 21.1 %collective-permute-start.8 = (bf16[64,2176]{1,0:T(8,128)(2,1)S(1)}, bf16[64,2176]{1,0:T(8,128)(2,1)S(1)}, u32[]{:S(2)}, u32[]{:S(2)}) collective-permute-start(bf16[64,2176]{1,0:T(8,128)(2,1)S(1)} %broadcast_select_fusion.refs_0_), channel_id=1, source_target_pairs={{0,1},{1,0},{2,3},{3,2},{4,5},{5,4},{6,7},{7,6},{8,9},{9,8},{10,11... | collective-permute-start | bytes 835592 | tf_op jit(solution)/shard_map/ppermute | solution.py:50
  41.5 21.0 %collective-permute-start.10 = (bf16[64,2176]{1,0:T(8,128)(2,1)S(1)}, bf16[64,2176]{1,0:T(8,128)(2,1)S(1)}, u32[]{:S(2)}, u32[]{:S(2)}) collective-permute-start(bf16[64,2176]{1,0:T(8,128)(2,1)S(1)} %collective-permute-done.9.refs_2_), channel_id=1, source_target_pairs={{0,1},{1,0},{2,3},{3,2},{4,5},{5,4},{6,7},{7,6},{8,9},{9,8},{10,11... | collective-permute-start | bytes 835592 | tf_op jit(solution)/shard_map/ppermute | solution.py:50
  48.7 17.6 %collective-permute-start.24 = (bf16[64,2176]{1,0:T(8,128)(2,1)S(1)}, bf16[64,2176]{1,0:T(8,128)(2,1)S(1)}, u32[]{:S(2)}, u32[]{:S(2)}) collective-permute-start(bf16[64,2176]{1,0:T(8,128)(2,1)S(1)} %collective-permute-done.23.refs_0_), channel_id=1, source_target_pairs={{0,1},{1,0},{2,3},{3,2},{4,5},{5,4},{6,7},{7,6},{8,9},{9,8},{10,11... | collective-permute-start | bytes 835592 | tf_op jit(solution)/shard_map/ppermute | solution.py:50
  48.7 19.1 %collective-permute-start.26 = (bf16[64,2176]{1,0:T(8,128)(2,1)S(1)}, bf16[64,2176]{1,0:T(8,128)(2,1)S(1)}, u32[]{:S(2)}, u32[]{:S(2)}) collective-permute-start(bf16[64,2176]{1,0:T(8,128)(2,1)S(1)} %collective-permute-done.25.refs_2_), channel_id=1, source_target_pairs={{0,1},{1,0},{2,3},{3,2},{4,5},{5,4},{6,7},{7,6},{8,9},{9,8},{10,11... | collective-permute-start | bytes 835592 | tf_op jit(solution)/shard_map/ppermute | solution.py:50
  73.3 9.3 %collective-permute-start.27 = (bf16[32,2048]{1,0:T(8,128)(2,1)S(1)}, bf16[32,2048]{1,0:T(8,128)(2,1)S(1)}, u32[]{:S(2)}, u32[]{:S(2)}) collective-permute-start(bf16[32,2048]{1,0:T(8,128)(2,1)S(1)} %get-tuple-element.46), channel_id=1, source_target_pairs={{0,1},{1,0},{2,3},{3,2},{4,5},{5,4},{6,7},{7,6},{8,9},{9,8},{10,11... | collective-permute-start | bytes 393224 | tf_op jit(solution)/shard_map/ppermute | solution.py:50
  81.0 15.2 %collective-permute-start.19 = (bf16[32,2048]{1,0:T(8,128)(2,1)S(1)}, bf16[32,2048]{1,0:T(8,128)(2,1)S(1)}, u32[]{:S(2)}, u32[]{:S(2)}) collective-permute-start(bf16[32,2048]{1,0:T(8,128)(2,1)S(1)} %get-tuple-element.41), channel_id=1, source_target_pairs={{0,1},{1,0},{2,3},{3,2},{4,5},{5,4},{6,7},{7,6},{8,9},{9,8},{10,11... | collective-permute-start | bytes 393224 | tf_op jit(solution)/shard_map/ppermute | solution.py:50
  81.0 16.8 %collective-permute-start.20 = (bf16[32,2048]{1,0:T(8,128)(2,1)S(1)}, bf16[32,2048]{1,0:T(8,128)(2,1)S(1)}, u32[]{:S(2)}, u32[]{:S(2)}) collective-permute-start(bf16[32,2048]{1,0:T(8,128)(2,1)S(1)} %get-tuple-element.42), channel_id=1, source_target_pairs={{0,2},{1,3},{2,0},{3,1},{4,6},{5,7},{6,4},{7,5},{8,10},{9,11},{10,... | collective-permute-start | bytes 393224 | tf_op jit(solution)/shard_map/ppermute | solution.py:50
  82.6 15.4 %collective-permute-start.21 = (bf16[32,2048]{1,0:T(8,128)(2,1)S(1)}, bf16[32,2048]{1,0:T(8,128)(2,1)S(1)}, u32[]{:S(2)}, u32[]{:S(2)}) collective-permute-start(bf16[32,2048]{1,0:T(8,128)(2,1)S(1)} %get-tuple-element.43), channel_id=1, source_target_pairs={{0,3},{1,2},{2,1},{3,0},{4,7},{5,6},{6,5},{7,4},{8,11},{9,10},{10,... | collective-permute-start | bytes 393224 | tf_op jit(solution)/shard_map/ppermute | solution.py:50
  83.6 18.2 %collective-permute-start.14 = (bf16[64,2048]{1,0:T(8,128)(2,1)S(1)}, bf16[64,2048]{1,0:T(8,128)(2,1)S(1)}, u32[]{:S(2)}, u32[]{:S(2)}) collective-permute-start(bf16[64,2048]{1,0:T(8,128)(2,1)S(1)} %shard_map.146), channel_id=1, source_target_pairs={{1,5},{3,7},{5,1},{7,3},{9,13},{11,15},{13,9},{15,11},{17,21},{19,... | collective-permute-start | bytes 786440 | tf_op jit(solution)/shard_map/ppermute | solution.py:342
  87.9 15.4 %collective-permute-start.1 = (bf16[256,256]{1,0:T(8,128)(2,1)S(1)}, bf16[256,256]{1,0:T(8,128)(2,1)S(1)}, u32[]{:S(2)}, u32[]{:S(2)}) collective-permute-start(bf16[256,256]{1,0:T(8,128)(2,1)S(1)} %get-tuple-element.29), channel_id=1, source_target_pairs={{0,1},{1,0},{2,3},{3,2},{4,5},{5,4},{6,7},{7,6},{8,9},{9,8},{10,11... | collective-permute-start | bytes 393224 | tf_op jit(solution)/shard_map/ppermute | solution.py:50
  97.8 11.0 %collective-permute-start.38 = (bf16[64,2048]{1,0:T(8,128)(2,1)S(1)}, bf16[64,2048]{1,0:T(8,128)(2,1)S(1)}, u32[]{:S(2)}, u32[]{:S(2)}) collective-permute-start(bf16[64,2048]{1,0:T(8,128)(2,1)S(1)} %shard_map.152), channel_id=1, source_target_pairs={{0,24},{1,29},{2,26},{3,31},{4,28},{5,25},{6,30},{7,27},{8,16},{9,... | collective-permute-start | bytes 786440 | tf_op jit(solution)/shard_map/ppermute | solution.py:342
  98.0 25.9 %collective-permute-start.30 = (bf16[64,2048]{1,0:T(8,128)(2,1)S(1)}, bf16[64,2048]{1,0:T(8,128)(2,1)S(1)}, u32[]{:S(2)}, u32[]{:S(2)}) collective-permute-start(bf16[64,2048]{1,0:T(8,128)(2,1)S(1)} %shard_map.150), channel_id=1, source_target_pairs={{0,16},{1,21},{2,18},{3,23},{4,20},{5,17},{6,22},{7,19},{8,24},{9,... | collective-permute-start | bytes 786440 | tf_op jit(solution)/shard_map/ppermute | solution.py:342
  101.8 22.1 %collective-permute-start.22 = (bf16[64,2048]{1,0:T(8,128)(2,1)S(1)}, bf16[64,2048]{1,0:T(8,128)(2,1)S(1)}, u32[]{:S(2)}, u32[]{:S(2)}) collective-permute-start(bf16[64,2048]{1,0:T(8,128)(2,1)S(1)} %shard_map.148), channel_id=1, source_target_pairs={{0,8},{1,13},{2,10},{3,15},{4,12},{5,9},{6,14},{7,11},{8,0},{9,5},... | collective-permute-start | bytes 786440 | tf_op jit(solution)/shard_map/ppermute | solution.py:342
  103.3 22.0 %collective-permute-start.3 = (bf16[256,256]{1,0:T(8,128)(2,1)S(1)}, bf16[256,256]{1,0:T(8,128)(2,1)S(1)}, u32[]{:S(2)}, u32[]{:S(2)}) collective-permute-start(bf16[256,256]{1,0:T(8,128)(2,1)S(1)} %get-tuple-element.31), channel_id=1, source_target_pairs={{0,3},{1,2},{2,1},{3,0},{4,7},{5,6},{6,5},{7,4},{8,11},{9,10},{10,... | collective-permute-start | bytes 393224 | tf_op jit(solution)/shard_map/ppermute | solution.py:50
  103.4 25.2 %collective-permute-start.39 = (bf16[64,2048]{1,0:T(8,128)(2,1)S(1)}, bf16[64,2048]{1,0:T(8,128)(2,1)S(1)}, u32[]{:S(2)}, u32[]{:S(2)}) collective-permute-start(bf16[64,2048]{1,0:T(8,128)(2,1)S(1)} %broadcast_select_fusion.1.refs_0_), channel_id=1, source_target_pairs={{0,1},{1,0},{2,3},{3,2},{4,5},{5,4},{6,7},{7,6},{8,9},{9,8},{10,11... | collective-permute-start | bytes 786440 | tf_op jit(solution)/shard_map/ppermute | solution.py:50
  108.8 19.8 %collective-permute-start.42 = (bf16[64,2048]{1,0:T(8,128)(2,1)S(1)}, bf16[64,2048]{1,0:T(8,128)(2,1)S(1)}, u32[]{:S(2)}, u32[]{:S(2)}) collective-permute-start(bf16[64,2048]{1,0:T(8,128)(2,1)S(1)} %collective-permute-done.38.refs_3_), channel_id=1, source_target_pairs={{0,1},{1,0},{2,3},{3,2},{4,5},{5,4},{6,7},{7,6},{8,9},{9,8},{10,11... | collective-permute-start | bytes 786440 | tf_op jit(solution)/shard_map/ppermute | solution.py:50
  (37 other events, 339.8 us)

commit v2 on v1

--- a/solution.py
+++ b/solution.py
@@ -74,14 +74,14 @@
         normed[at, :width] = (wide * scale * gain[...]).astype(BF16)
         return carry
 
-    lax.fori_loop(0, tokens // step, rows, 0)
-
-
-def ranks(sizes, ids, me):
+    lax.fori_loop(0, tokens // step, rows, 0, unroll=True)
+
+
+def ranks(sizes, route, me):
     groups, members, per_group, _ = sizes
-    tokens = ids.shape[1]
+    tokens = route.shape[1]
     experts = -(-groups * members // 16) * 16
-    first, second = ids[0:1, :], ids[1:2, :]
+    first, second = (route[k : k + 1, :].astype(jnp.int32) for k in range(2))
     before = (iota((tokens, tokens), 0) < iota((tokens, tokens), 1)).astype(BF16)
     lane = iota((experts, tokens), 0)
     one, two = lane == first, lane == second
@@ -94,14 +94,14 @@
     return rank_one, rank_two, (mask // 2) * (2 * per_group) + rank.astype(jnp.int32), jnp.bitwise_and(mask, 1)
 
 
-def route_rows(sizes, ids, weights, normed, me):
+def route_rows(sizes, route, normed, me):
     _, members, _, width = sizes
     tokens = normed.shape[0]
-    first, second = ids[0:1, :], ids[1:2, :]
-    rank_one, rank_two, base, odd = ranks(sizes, ids, me)
+    first, second = (route[k : k + 1, :].astype(jnp.int32) for k in range(2))
+    rank_one, rank_two, base, odd = ranks(sizes, route, me)
     parts = []
     for k in range(2):
-        left = weights[k : k + 1, :]
+        left = route[2 + k : 3 + k, :]
         for _ in range(3):
             part = left.astype(BF16).astype(F32)
             parts.append(part)
@@ -118,23 +118,23 @@
     return base, odd
 
 
-def own_body(sizes, where, x, ids, weights, gain, normed, place):
-    base, odd = route_rows(sizes, ids, weights, normed, where[0])
+def own_body(sizes, where, x, route, gain, normed, place):
+    base, odd = route_rows(sizes, route, normed, where[0])
     place[...] = jnp.broadcast_to(jnp.where(odd == where[2], base, -1), place.shape)
     norm_rows(x, gain, normed, sizes[3])
 
 
-def back_body(sizes, where, ids, pos):
+def back_body(sizes, where, route, pos):
     groups, _, per_group, _ = sizes
-    _, _, base, odd = ranks(sizes, ids, where[0])
+    _, _, base, odd = ranks(sizes, route, where[0])
     back = jnp.where(odd == where[2], base, groups * per_group + base + per_group).astype(F32)
     pos[...] = jnp.broadcast_to(back, (pos.shape[1], pos.shape[0])).T
 
 
-def prep_body(sizes, where, own, place_own, x_mate, ids_mate, weights_mate, gain, *refs):
+def prep_body(sizes, where, own, place_own, x_mate, route_mate, gain, *refs):
     groups, _, per_group, width = sizes
     chunks, mate = refs[:-1], refs[-1]
-    base, odd = route_rows(sizes, ids_mate, weights_mate, mate, where[0])
+    base, odd = route_rows(sizes, route_mate, mate, where[0])
     norm_rows(x_mate, gain, mate, width)
     place_mate = jnp.where(odd == where[2], base + per_group, -1)
     total = groups * per_group
@@ -151,7 +151,7 @@
             ref[:, cols] = out[k * size : (k + 1) * size]
         return carry
 
-    lax.fori_loop(0, 4, columns, 0)
+    lax.fori_loop(0, 4, columns, 0, unroll=True)
     out = dot(pick, jnp.concatenate([own[:, width:], mate[:, width:]], axis=0)).astype(BF16)
     for k, ref in enumerate(chunks):
         ref[:, width:] = out[k * size : (k + 1) * size]
@@ -167,17 +167,17 @@
     span = count * 2 * per_expert
     block = 512
     pick_row = (iota((META, LANES), 0) == iota((META, LANES), 1)).astype(BF16)
-    for m in range(members):
-        lanes = jnp.concatenate([r[:, width:] for r in landed[m]], axis=0)
-        meta = dot_nt(pick_row, lanes).astype(jnp.int32)
-        n = iota((1, count * size), 1)
-        base = (n // size) * (2 * per_expert) + ((n % size) // per_group) * per_expert
-        at = jnp.where(meta[0:1] == me, base + meta[1:2], jnp.where(meta[2:3] == me, base + meta[3:4], -1))
-        pick = (iota((span, count * size), 0) == at).astype(BF16)
-        for n in range(width // block):
-            cols = slice(n * block, (n + 1) * block)
-            value = jnp.concatenate([r[:, cols] for r in landed[m]], axis=0)
-            rows_x[m * span : (m + 1) * span, cols] = dot(pick, value).astype(BF16)
+    flat = [r for one in landed for r in one]
+    meta = dot_nt(pick_row, jnp.concatenate([r[:, width:] for r in flat], axis=0)).astype(jnp.int32)
+    total = members * count * size
+    n = iota((1, total), 1)
+    chunk = (n // (count * size)) * count + (n % (count * size)) // size
+    base = chunk * (2 * per_expert) + ((n % size) // per_group) * per_expert
+    at = jnp.where(meta[0:1] == me, base + meta[1:2], jnp.where(meta[2:3] == me, base + meta[3:4], -1))
+    pick = (iota((members * span, total), 0) == at).astype(BF16)
+    for n in range(width // block):
+        cols = slice(n * block, (n + 1) * block)
+        rows_x[:, cols] = dot(pick, jnp.concatenate([r[:, cols] for r in flat], axis=0)).astype(BF16)
     gated = dot(rows_x[...], gate[...])
     upper = dot(rows_x[...], up[...])
     hidden[...] = (gated / (1.0 + jnp.exp(-gated)) * upper).astype(BF16)
@@ -307,15 +307,15 @@
     reach = conv_taps.shape[0] - 1
 
     x_mate = swap(moe_in, "tp", 1)
-    ids, ids_mate = route_ids.T, swap(route_ids.T, "tp", 1)
-    weights, weights_mate = route_weight.T, swap(route_weight.T, "tp", 1)
+    route = jnp.concatenate([route_ids.astype(F32), route_weight], axis=1).T
+    route_mate = swap(route, "tp", 1)
     gain = moe_gain.reshape(1, width)
     sizes_all = (groups, members, per_group, width)
     normed, place = call(
         functools.partial(own_body, sizes_all),
         [jax.ShapeDtypeStruct((tokens, full), BF16), jax.ShapeDtypeStruct((8, tokens), jnp.int32)],
-        [SMEM] + [VMEM] * 4,
-        (where, moe_in, ids, weights, gain),
+        [SMEM] + [VMEM] * 3,
+        (where, moe_in, route, gain),
         [],
         6 << 30,
         16,
@@ -323,8 +323,8 @@
     leaving = call(
         functools.partial(prep_body, sizes_all),
         [jax.ShapeDtypeStruct((size, full), BF16)] * n_chunks,
-        [SMEM] + [VMEM] * 6,
-        (where, normed, place, x_mate, ids_mate, weights_mate, gain),
+        [SMEM] + [VMEM] * 5,
+        (where, normed, place, x_mate, route_mate, gain),
         [pltpu.VMEM((tokens, full), BF16)],
         20 << 30,
         16,
@@ -411,7 +411,7 @@
         functools.partial(back_body, sizes_all),
         jax.ShapeDtypeStruct((tokens, LANES), F32),
         [SMEM, VMEM],
-        (where, ids),
+        (where, route),
         [],
         20 << 30,
         8,

time: 131 us -> 128 us (0.977)
  Pallas kernels: 29.6 us -> 26 us
  waiting for transfers between devices: 48.9 us -> 50.6 us
  local copies, waits for them, and re-layouts: 9.9 us -> 8.53 us
  other arithmetic: 0.14 us -> 1.51 us
    pallas_call x14, Pallas kernels: 29.6 us -> 26 us  [call(): pl.pallas_call(body, out_shape=outs, in_specs=specs, out_specs=jax.tree.m...]
    unnamed x32 -> x26, local copies, waits for them, and re-layouts: 9.88 us -> 8.52 us
    ppermute x34 -> x33, waiting for transfers between devices: 8.33 us -> 9.61 us  [swap(): return lax.ppermute(value, axis, [(i, i ^ mask) for i in range(count)])]
    ppermute x34 -> x33, starting transfers between devices: 25.9 us -> 25.3 us  [swap(): return lax.ppermute(value, axis, [(i, i ^ mask) for i in range(count)])]
  transfers between devices with their start and end apart: 43 -> 42, of which waited for: 7 -> 7; matrix products, arithmetic and copies ran while one was open for 0% -> 1% of each run, Pallas kernels for 19% -> 18%
where the time goes in v2:
time: 128 us; the launch traced here: 127 us
  waiting for transfers between devices  50.6 us (40%)
  starting transfers between devices  39.5 us (31%)
  Pallas kernels  26 us (20%)
  local copies, waits for them, and re-layouts  8.53 us (7%)
  other arithmetic  1.51 us (1%)
    ppermute x8, waiting for transfers between devices, across(): got = lax.ppermute(value, ('ep', 'tp'), pairs)  40.9 us
    pallas_call x14, Pallas kernels, call(): pl.pallas_call(body, out_shape=outs, in_specs=specs, out_specs=jax.tree.m...  26 us
    ppermute x33, starting transfers between devices, swap(): return lax.ppermute(value, axis, [(i, i ^ mask) for i in range(count)])  25.3 us
    ppermute x8, starting transfers between devices, across(): got = lax.ppermute(value, ('ep', 'tp'), pairs)  11.6 us
    ppermute x33, waiting for transfers between devices, swap(): return lax.ppermute(value, axis, [(i, i ^ mask) for i in range(count)])  9.61 us
    unnamed x26, local copies, waits for them, and re-layouts  8.52 us
    ppermute x1, starting transfers between devices, shards(): edge = lax.ppermute(edge, 'ep', [(i, i + 1) for i in range(groups - 1)])  2.62 us
  transfers between devices with their start and end apart: 42, of which 7 were waited for; matrix products, arithmetic and copies ran while one was open for 1% of the time, Pallas kernels for 18%

profile of v2, /device:TPU:0, one launch (start us, length us, event | category | flops | bytes accessed | tf_op | source)
XLA Modules:
  0.0 127.2 jit_solution(13899411974570400854)
XLA Ops:
  5.9 1.8 %shard_map.144 = (bf16[64,2176]{1,0:T(8,128)(2,1)S(1)}, bf16[64,2176]{1,0:T(8,128)(2,1)S(1)}, bf16[64,2176]{1,0:T(8,128)(2,1)S(1)}, bf16[64,2176]{1,0:T(8,128)(2,1)S(1)}) custom-call(s32[3]{0:T(128)S(1)} %pad_add_fusion.where, bf16[256,2176]{1,0:T(8,128)(2,1)S(1)} %get-tuple-element.32.own, s32[8,256]{1,0:T(8,128)S(1)} %get-tuple-element.33.place_own, ...), custom_call_target="tpu_custom_call" | custom-call | flops 21474836480 | bytes 1048576 | tf_op jit(solution)/shard_map/pallas_call | solution.py:37
  7.7 5.1 %collective-permute-start.30 = (bf16[64,2176]{1,0:T(8,128)(2,1)S(1)}, bf16[64,2176]{1,0:T(8,128)(2,1)S(1)}, u32[]{:S(2)}, u32[]{:S(2)}) collective-permute-start(bf16[64,2176]{1,0:T(8,128)(2,1)S(1)} %get-tuple-element.49), channel_id=1, source_target_pairs={{0,24},{1,29},{2,26},{3,31},{4,28},{5,25},{6,30},{7,27},{8,16},{9,... | collective-permute-start | bytes 835592 | tf_op jit(solution)/shard_map/ppermute | solution.py:342
  14.2 6.2 %collective-permute-done.30.refs_0_ = bf16[64,2176]{1,0:T(8,128)(2,1)S(1)} collective-permute-done((bf16[64,2176]{1,0:T(8,128)(2,1)S(1)}, bf16[64,2176]{1,0:T(8,128)(2,1)S(1)}, u32[]{:S(2)}, u32[]{:S(2)}) %collective-permute-start.30) | collective-permute-done | bytes 278560 | tf_op jit(solution)/shard_map/ppermute | solution.py:342
  20.4 1.9 %collective-permute-start.32 = (bf16[64,2176]{1,0:T(8,128)(2,1)S(1)}, bf16[64,2176]{1,0:T(8,128)(2,1)S(1)}, u32[]{:S(2)}, u32[]{:S(2)}) collective-permute-start(bf16[64,2176]{1,0:T(8,128)(2,1)S(1)} %collective-permute-done.30.refs_0_), channel_id=1, source_target_pairs={{0,2},{1,3},{2,0},{3,1},{4,6},{5,7},{6,4},{7,5},{8,10},{9,11},{10,... | collective-permute-start | bytes 835592 | tf_op jit(solution)/shard_map/ppermute | solution.py:50
  22.5 15.2 %collective-permute-done.22.refs_0_ = bf16[64,2176]{1,0:T(8,128)(2,1)S(1)} collective-permute-done((bf16[64,2176]{1,0:T(8,128)(2,1)S(1)}, bf16[64,2176]{1,0:T(8,128)(2,1)S(1)}, u32[]{:S(2)}, u32[]{:S(2)}) %collective-permute-start.22) | collective-permute-done | bytes 278560 | tf_op jit(solution)/shard_map/ppermute | solution.py:342
  40.3 6.9 %collective-permute-done.24.refs_2_ = bf16[64,2176]{1,0:T(8,128)(2,1)S(1)} collective-permute-done((bf16[64,2176]{1,0:T(8,128)(2,1)S(1)}, bf16[64,2176]{1,0:T(8,128)(2,1)S(1)}, u32[]{:S(2)}, u32[]{:S(2)}) %collective-permute-start.24) | collective-permute-done | bytes 278560 | tf_op jit(solution)/shard_map/ppermute | solution.py:50
  47.7 2.2 %copy-done = bf16[1,2048,1024]{2,1,0:T(8,128)(2,1)S(1)} copy-done((bf16[1,2048,1024]{2,1,0:T(8,128)(2,1)S(1)}, bf16[1,2048,1024]{2,1,0:T(8,128)(2,1)}, u32[]{:S(2)}) %copy-start) | copy-done | bytes 4194328
  49.9 2.2 %copy-done.2 = bf16[1,2048,1024]{2,1,0:T(8,128)(2,1)S(1)} copy-done((bf16[1,2048,1024]{2,1,0:T(8,128)(2,1)S(1)}, bf16[1,2048,1024]{2,1,0:T(8,128)(2,1)}, u32[]{:S(2)}) %copy-start.2) | copy-done | bytes 4194328
  52.1 2.2 %copy-done.3 = bf16[1,1024,2048]{2,1,0:T(8,128)(2,1)S(1)} copy-done((bf16[1,1024,2048]{2,1,0:T(8,128)(2,1)S(1)}, bf16[1,1024,2048]{2,1,0:T(8,128)(2,1)}, u32[]{:S(2)}) %copy-start.3) | copy-done | bytes 4194328
  54.3 2.7 %shard_map.151 = (bf16[32,2048]{1,0:T(8,128)(2,1)S(1)}, bf16[32,2048]{1,0:T(8,128)(2,1)S(1)}, bf16[32,2048]{1,0:T(8,128)(2,1)S(1)}, bf16[32,2048]{1,0:T(8,128)(2,1)S(1)}) custom-call(s32[3]{0:T(128)S(1)} %pad_add_fusion.where, bf16[64,2176]{1,0:T(8,128)(2,1)S(1)} %collective-permute-done.30.refs_0_, bf16[64,2176]{1,0:T(8,128)(2,1)S(1)} %collective-permute-done.31.refs_1_, ...), custom_call_target="tpu_custom_call" | custom-call | flops 1610612736 | bytes 1048576 | tf_op jit(solution)/shard_map/pallas_call | solution.py:37
  57.0 2.6 %collective-permute-start = (bf16[16,256]{1,0:T(8,128)(2,1)S(1)}, bf16[16,256]{1,0:T(8,128)(2,1)S(1)}, u32[]{:S(2)}, u32[]{:S(2)}) collective-permute-start(bf16[16,256]{1,0:T(8,128)(2,1)S(1)} %pad_maximum_fusion), channel_id=1, source_target_pairs={{0,4},{4,8},{8,12},{12,16},{16,20},{20,24},{24,28},{1,5},{5,9},{9,... | collective-permute-start | bytes 24584 | tf_op jit(solution)/shard_map/ppermute | solution.py:333
  60.3 2.7 %shard_map.145 = (bf16[32,2048]{1,0:T(8,128)(2,1)S(1)}, bf16[32,2048]{1,0:T(8,128)(2,1)S(1)}, bf16[32,2048]{1,0:T(8,128)(2,1)S(1)}, bf16[32,2048]{1,0:T(8,128)(2,1)S(1)}) custom-call(s32[3]{0:T(128)S(1)} %pad_add_fusion.where, bf16[64,2176]{1,0:T(8,128)(2,1)S(1)} %broadcast_select_fusion.refs_0_, bf16[64,2176]{1,0:T(8,128)(2,1)S(1)} %collective-permute-done.7.refs_1_, ...), custom_call_target="tpu_custom_call" | custom-call | flops 1610612736 | bytes 1048576 | tf_op jit(solution)/shard_map/pallas_call | solution.py:37
  64.9 2.7 %shard_map.149 = (bf16[32,2048]{1,0:T(8,128)(2,1)S(1)}, bf16[32,2048]{1,0:T(8,128)(2,1)S(1)}, bf16[32,2048]{1,0:T(8,128)(2,1)S(1)}, bf16[32,2048]{1,0:T(8,128)(2,1)S(1)}) custom-call(s32[3]{0:T(128)S(1)} %pad_add_fusion.where, bf16[64,2176]{1,0:T(8,128)(2,1)S(1)} %collective-permute-done.22.refs_0_, bf16[64,2176]{1,0:T(8,128)(2,1)S(1)} %collective-permute-done.23.refs_1_, ...), custom_call_target="tpu_custom_call" | custom-call | flops 1610612736 | bytes 1048576 | tf_op jit(solution)/shard_map/pallas_call | solution.py:37
  72.9 2.7 %shard_map.147 = (bf16[32,2048]{1,0:T(8,128)(2,1)S(1)}, bf16[32,2048]{1,0:T(8,128)(2,1)S(1)}, bf16[32,2048]{1,0:T(8,128)(2,1)S(1)}, bf16[32,2048]{1,0:T(8,128)(2,1)S(1)}) custom-call(s32[3]{0:T(128)S(1)} %pad_add_fusion.where, bf16[64,2176]{1,0:T(8,128)(2,1)S(1)} %collective-permute-done.14.refs_0_, bf16[64,2176]{1,0:T(8,128)(2,1)S(1)} %collective-permute-done.15.refs_1_, ...), custom_call_target="tpu_custom_call" | custom-call | flops 1610612736 | bytes 1048576 | tf_op jit(solution)/shard_map/pallas_call | solution.py:37
  77.4 1.6 %collective-permute-start.19 = (bf16[32,2048]{1,0:T(8,128)(2,1)S(1)}, bf16[32,2048]{1,0:T(8,128)(2,1)S(1)}, u32[]{:S(2)}, u32[]{:S(2)}) collective-permute-start(bf16[32,2048]{1,0:T(8,128)(2,1)S(1)} %get-tuple-element.42), channel_id=1, source_target_pairs={{0,2},{1,3},{2,0},{3,1},{4,6},{5,7},{6,4},{7,5},{8,10},{9,11},{10,... | collective-permute-start | bytes 393224 | tf_op jit(solution)/shard_map/ppermute | solution.py:50
  79.2 1.5 %collective-permute-done.27.refs_3_ = bf16[32,2048]{1,0:T(8,128)(2,1)S(1)} collective-permute-done((bf16[32,2048]{1,0:T(8,128)(2,1)S(1)}, bf16[32,2048]{1,0:T(8,128)(2,1)S(1)}, u32[]{:S(2)}, u32[]{:S(2)}) %collective-permute-start.27) | collective-permute-done | bytes 131104 | tf_op jit(solution)/shard_map/ppermute | solution.py:50
  81.5 2.4 %shard_map.140 = (bf16[256,256]{1,0:T(8,128)(2,1)S(1)}, bf16[256,256]{1,0:T(8,128)(2,1)S(1)}, bf16[256,256]{1,0:T(8,128)(2,1)S(1)}, bf16[256,256]{1,0:T(8,128)(2,1)S(1)}) custom-call(s32[3]{0:T(128)S(1)} %pad_add_fusion.where, bf16[16,256]{1,0:T(8,128)(2,1)S(1)} %collective-permute-done.edge, bf16[1024,256]{1,0:T(8,128)(2,1)S(1)} %copy-done.6, ...), custom_call_target="tpu_custom_call" | custom-call | flops 21474836480 | bytes 1048576 | tf_op jit(solution)/shard_map/pallas_call | solution.py:37
  84.9 7.5 %collective-permute-start.1 = (bf16[256,256]{1,0:T(8,128)(2,1)S(1)}, bf16[256,256]{1,0:T(8,128)(2,1)S(1)}, u32[]{:S(2)}, u32[]{:S(2)}) collective-permute-start(bf16[256,256]{1,0:T(8,128)(2,1)S(1)} %get-tuple-element.29), channel_id=1, source_target_pairs={{0,1},{1,0},{2,3},{3,2},{4,5},{5,4},{6,7},{7,6},{8,9},{9,8},{10,11... | collective-permute-start | bytes 393224 | tf_op jit(solution)/shard_map/ppermute | solution.py:50
  93.4 1.6 %collective-permute-start.2 = (bf16[256,256]{1,0:T(8,128)(2,1)S(1)}, bf16[256,256]{1,0:T(8,128)(2,1)S(1)}, u32[]{:S(2)}, u32[]{:S(2)}) collective-permute-start(bf16[256,256]{1,0:T(8,128)(2,1)S(1)} %get-tuple-element.30), channel_id=1, source_target_pairs={{0,2},{1,3},{2,0},{3,1},{4,6},{5,7},{6,4},{7,5},{8,10},{9,11},{10,... | collective-permute-start | bytes 393224 | tf_op jit(solution)/shard_map/ppermute | solution.py:50
  95.3 2.7 %collective-permute-start.29 = (bf16[64,2048]{1,0:T(8,128)(2,1)S(1)}, bf16[64,2048]{1,0:T(8,128)(2,1)S(1)}, u32[]{:S(2)}, u32[]{:S(2)}) collective-permute-start(bf16[64,2048]{1,0:T(8,128)(2,1)S(1)} %shard_map.150), channel_id=1, source_target_pairs={{0,16},{1,21},{2,18},{3,23},{4,20},{5,17},{6,22},{7,19},{8,24},{9,... | collective-permute-start | bytes 786440 | tf_op jit(solution)/shard_map/ppermute | solution.py:342
  101.1 4.9 %collective-permute-done.37.refs_3_ = bf16[64,2048]{1,0:T(8,128)(2,1)S(1)} collective-permute-done((bf16[64,2048]{1,0:T(8,128)(2,1)S(1)}, bf16[64,2048]{1,0:T(8,128)(2,1)S(1)}, u32[]{:S(2)}, u32[]{:S(2)}) %collective-permute-start.37) | collective-permute-done | bytes 262176 | tf_op jit(solution)/shard_map/ppermute | solution.py:342
  106.0 14.7 %collective-permute-done.29.refs_2_ = bf16[64,2048]{1,0:T(8,128)(2,1)S(1)} collective-permute-done((bf16[64,2048]{1,0:T(8,128)(2,1)S(1)}, bf16[64,2048]{1,0:T(8,128)(2,1)S(1)}, u32[]{:S(2)}, u32[]{:S(2)}) %collective-permute-start.29) | collective-permute-done | bytes 262176 | tf_op jit(solution)/shard_map/ppermute | solution.py:342
  122.1 3.3 %shard_map.141 = bf16[256,2048]{1,0:T(8,128)(2,1)} custom-call(s32[3]{0:T(128)S(1)} %pad_add_fusion.where, bf16[1024,2048]{1,0:T(8,128)(2,1)S(1)} %copy-done.4, bf16[256,256]{1,0:T(8,128)(2,1)S(1)} %get-tuple-element.28.refs_0_, bf16[256,256]{1,0:T(8,128)(2,1)S(1)} %collective-permute-done.1.refs_1_, bf16[256,256]{1,0:T(8,128)(2,1)S(1)} %collective-permute-done.2.refs_2_, ...), custom_call_target="tpu_custom_call" | custom-call | flops 1073741824 | bytes 1048576 | tf_op jit(solution)/shard_map/pallas_call | solution.py:37
  125.4 1.7 %shard_map.153 = bf16[256,2048]{1,0:T(8,128)(2,1)} custom-call(f32[256,128]{1,0:T(8,128)S(1)} %shard_map.142.pos, bf16[64,2048]{1,0:T(8,128)(2,1)S(1)} %broadcast_select_fusion.1.refs_0_, bf16[64,2048]{1,0:T(8,128)(2,1)S(1)} %collective-permute-done.21.refs_1_, bf16[64,2048]{1,0:T(8,128)(2,1)S(1)} %collective-permute-done.29.refs_2_, ...), custom_call_target="tpu_custom_call" | custom-call | flops 536870912 | bytes 1048576 | tf_op jit(solution)/shard_map/pallas_call | solution.py:37
  (110 shorter events, 27.0 us)
Async XLA Ops:
  7.7 12.7 %collective-permute-start.30 = (bf16[64,2176]{1,0:T(8,128)(2,1)S(1)}, bf16[64,2176]{1,0:T(8,128)(2,1)S(1)}, u32[]{:S(2)}, u32[]{:S(2)}) collective-permute-start(bf16[64,2176]{1,0:T(8,128)(2,1)S(1)} %get-tuple-element.49), channel_id=1, source_target_pairs={{0,24},{1,29},{2,26},{3,31},{4,28},{5,25},{6,30},{7,27},{8,16},{9,... | collective-permute-start | bytes 835592 | tf_op jit(solution)/shard_map/ppermute | solution.py:342
  12.9 9.4 %collective-permute-start.6 = (bf16[64,2176]{1,0:T(8,128)(2,1)S(1)}, bf16[64,2176]{1,0:T(8,128)(2,1)S(1)}, u32[]{:S(2)}, u32[]{:S(2)}) collective-permute-start(bf16[64,2176]{1,0:T(8,128)(2,1)S(1)} %get-tuple-element.34), channel_id=1, source_target_pairs={{1,5},{3,7},{5,1},{7,3},{9,13},{11,15},{13,9},{15,11},{17,21},{19,... | collective-permute-start | bytes 835592 | tf_op jit(solution)/shard_map/ppermute | solution.py:342
  13.5 24.1 %collective-permute-start.22 = (bf16[64,2176]{1,0:T(8,128)(2,1)S(1)}, bf16[64,2176]{1,0:T(8,128)(2,1)S(1)}, u32[]{:S(2)}, u32[]{:S(2)}) collective-permute-start(bf16[64,2176]{1,0:T(8,128)(2,1)S(1)} %get-tuple-element.44), channel_id=1, source_target_pairs={{0,16},{1,21},{2,18},{3,23},{4,20},{5,17},{6,22},{7,19},{8,24},{9,... | collective-permute-start | bytes 835592 | tf_op jit(solution)/shard_map/ppermute | solution.py:342
  13.6 25.6 %collective-permute-start.14 = (bf16[64,2176]{1,0:T(8,128)(2,1)S(1)}, bf16[64,2176]{1,0:T(8,128)(2,1)S(1)}, u32[]{:S(2)}, u32[]{:S(2)}) collective-permute-start(bf16[64,2176]{1,0:T(8,128)(2,1)S(1)} %get-tuple-element.39), channel_id=1, source_target_pairs={{0,8},{1,13},{2,10},{3,15},{4,12},{5,9},{6,14},{7,11},{8,0},{9,5},... | collective-permute-start | bytes 835592 | tf_op jit(solution)/shard_map/ppermute | solution.py:342
  20.4 18.8 %collective-permute-start.32 = (bf16[64,2176]{1,0:T(8,128)(2,1)S(1)}, bf16[64,2176]{1,0:T(8,128)(2,1)S(1)}, u32[]{:S(2)}, u32[]{:S(2)}) collective-permute-start(bf16[64,2176]{1,0:T(8,128)(2,1)S(1)} %collective-permute-done.30.refs_0_), channel_id=1, source_target_pairs={{0,2},{1,3},{2,0},{3,1},{4,6},{5,7},{6,4},{7,5},{8,10},{9,11},{10,... | collective-permute-start | bytes 835592 | tf_op jit(solution)/shard_map/ppermute | solution.py:50
  22.3 17.5 %collective-permute-start.31 = (bf16[64,2176]{1,0:T(8,128)(2,1)S(1)}, bf16[64,2176]{1,0:T(8,128)(2,1)S(1)}, u32[]{:S(2)}, u32[]{:S(2)}) collective-permute-start(bf16[64,2176]{1,0:T(8,128)(2,1)S(1)} %collective-permute-done.30.refs_0_), channel_id=1, source_target_pairs={{0,1},{1,0},{2,3},{3,2},{4,5},{5,4},{6,7},{7,6},{8,9},{9,8},{10,11... | collective-permute-start | bytes 835592 | tf_op jit(solution)/shard_map/ppermute | solution.py:50
  22.3 17.6 %collective-permute-start.8 = (bf16[64,2176]{1,0:T(8,128)(2,1)S(1)}, bf16[64,2176]{1,0:T(8,128)(2,1)S(1)}, u32[]{:S(2)}, u32[]{:S(2)}) collective-permute-start(bf16[64,2176]{1,0:T(8,128)(2,1)S(1)} %broadcast_select_fusion.refs_0_), channel_id=1, source_target_pairs={{0,2},{1,3},{2,0},{3,1},{4,6},{5,7},{6,4},{7,5},{8,10},{9,11},{10,... | collective-permute-start | bytes 835592 | tf_op jit(solution)/shard_map/ppermute | solution.py:50
  37.7 9.5 %collective-permute-start.24 = (bf16[64,2176]{1,0:T(8,128)(2,1)S(1)}, bf16[64,2176]{1,0:T(8,128)(2,1)S(1)}, u32[]{:S(2)}, u32[]{:S(2)}) collective-permute-start(bf16[64,2176]{1,0:T(8,128)(2,1)S(1)} %collective-permute-done.22.refs_0_), channel_id=1, source_target_pairs={{0,2},{1,3},{2,0},{3,1},{4,6},{5,7},{6,4},{7,5},{8,10},{9,11},{10,... | collective-permute-start | bytes 835592 | tf_op jit(solution)/shard_map/ppermute | solution.py:50
  39.2 17.8 %collective-permute-start.16 = (bf16[64,2176]{1,0:T(8,128)(2,1)S(1)}, bf16[64,2176]{1,0:T(8,128)(2,1)S(1)}, u32[]{:S(2)}, u32[]{:S(2)}) collective-permute-start(bf16[64,2176]{1,0:T(8,128)(2,1)S(1)} %collective-permute-done.14.refs_0_), channel_id=1, source_target_pairs={{0,2},{1,3},{2,0},{3,1},{4,6},{5,7},{6,4},{7,5},{8,10},{9,11},{10,... | collective-permute-start | bytes 835592 | tf_op jit(solution)/shard_map/ppermute | solution.py:50
  39.8 19.9 %collective-permute-start.7 = (bf16[64,2176]{1,0:T(8,128)(2,1)S(1)}, bf16[64,2176]{1,0:T(8,128)(2,1)S(1)}, u32[]{:S(2)}, u32[]{:S(2)}) collective-permute-start(bf16[64,2176]{1,0:T(8,128)(2,1)S(1)} %broadcast_select_fusion.refs_0_), channel_id=1, source_target_pairs={{0,1},{1,0},{2,3},{3,2},{4,5},{5,4},{6,7},{7,6},{8,9},{9,8},{10,11... | collective-permute-start | bytes 835592 | tf_op jit(solution)/shard_map/ppermute | solution.py:50
  40.0 19.8 %collective-permute-start.9 = (bf16[64,2176]{1,0:T(8,128)(2,1)S(1)}, bf16[64,2176]{1,0:T(8,128)(2,1)S(1)}, u32[]{:S(2)}, u32[]{:S(2)}) collective-permute-start(bf16[64,2176]{1,0:T(8,128)(2,1)S(1)} %collective-permute-done.8.refs_2_), channel_id=1, source_target_pairs={{0,1},{1,0},{2,3},{3,2},{4,5},{5,4},{6,7},{7,6},{8,9},{9,8},{10,11... | collective-permute-start | bytes 835592 | tf_op jit(solution)/shard_map/ppermute | solution.py:50
  47.2 15.9 %collective-permute-start.23 = (bf16[64,2176]{1,0:T(8,128)(2,1)S(1)}, bf16[64,2176]{1,0:T(8,128)(2,1)S(1)}, u32[]{:S(2)}, u32[]{:S(2)}) collective-permute-start(bf16[64,2176]{1,0:T(8,128)(2,1)S(1)} %collective-permute-done.22.refs_0_), channel_id=1, source_target_pairs={{0,1},{1,0},{2,3},{3,2},{4,5},{5,4},{6,7},{7,6},{8,9},{9,8},{10,11... | collective-permute-start | bytes 835592 | tf_op jit(solution)/shard_map/ppermute | solution.py:50
  47.2 17.5 %collective-permute-start.25 = (bf16[64,2176]{1,0:T(8,128)(2,1)S(1)}, bf16[64,2176]{1,0:T(8,128)(2,1)S(1)}, u32[]{:S(2)}, u32[]{:S(2)}) collective-permute-start(bf16[64,2176]{1,0:T(8,128)(2,1)S(1)} %collective-permute-done.24.refs_2_), channel_id=1, source_target_pairs={{0,1},{1,0},{2,3},{3,2},{4,5},{5,4},{6,7},{7,6},{8,9},{9,8},{10,11... | collective-permute-start | bytes 835592 | tf_op jit(solution)/shard_map/ppermute | solution.py:50
  77.4 16.0 %collective-permute-start.18 = (bf16[32,2048]{1,0:T(8,128)(2,1)S(1)}, bf16[32,2048]{1,0:T(8,128)(2,1)S(1)}, u32[]{:S(2)}, u32[]{:S(2)}) collective-permute-start(bf16[32,2048]{1,0:T(8,128)(2,1)S(1)} %get-tuple-element.41), channel_id=1, source_target_pairs={{0,1},{1,0},{2,3},{3,2},{4,5},{5,4},{6,7},{7,6},{8,9},{9,8},{10,11... | collective-permute-start | bytes 393224 | tf_op jit(solution)/shard_map/ppermute | solution.py:50
  77.4 17.6 %collective-permute-start.19 = (bf16[32,2048]{1,0:T(8,128)(2,1)S(1)}, bf16[32,2048]{1,0:T(8,128)(2,1)S(1)}, u32[]{:S(2)}, u32[]{:S(2)}) collective-permute-start(bf16[32,2048]{1,0:T(8,128)(2,1)S(1)} %get-tuple-element.42), channel_id=1, source_target_pairs={{0,2},{1,3},{2,0},{3,1},{4,6},{5,7},{6,4},{7,5},{8,10},{9,11},{10,... | collective-permute-start | bytes 393224 | tf_op jit(solution)/shard_map/ppermute | solution.py:50
  79.0 16.3 %collective-permute-start.20 = (bf16[32,2048]{1,0:T(8,128)(2,1)S(1)}, bf16[32,2048]{1,0:T(8,128)(2,1)S(1)}, u32[]{:S(2)}, u32[]{:S(2)}) collective-permute-start(bf16[32,2048]{1,0:T(8,128)(2,1)S(1)} %get-tuple-element.43), channel_id=1, source_target_pairs={{0,3},{1,2},{2,1},{3,0},{4,7},{5,6},{6,5},{7,4},{8,11},{9,10},{10,... | collective-permute-start | bytes 393224 | tf_op jit(solution)/shard_map/ppermute | solution.py:50
  80.8 18.2 %collective-permute-start.13 = (bf16[64,2048]{1,0:T(8,128)(2,1)S(1)}, bf16[64,2048]{1,0:T(8,128)(2,1)S(1)}, u32[]{:S(2)}, u32[]{:S(2)}) collective-permute-start(bf16[64,2048]{1,0:T(8,128)(2,1)S(1)} %shard_map.146), channel_id=1, source_target_pairs={{1,5},{3,7},{5,1},{7,3},{9,13},{11,15},{13,9},{15,11},{17,21},{19,... | collective-permute-start | bytes 786440 | tf_op jit(solution)/shard_map/ppermute | solution.py:342
  84.9 15.6 %collective-permute-start.1 = (bf16[256,256]{1,0:T(8,128)(2,1)S(1)}, bf16[256,256]{1,0:T(8,128)(2,1)S(1)}, u32[]{:S(2)}, u32[]{:S(2)}) collective-permute-start(bf16[256,256]{1,0:T(8,128)(2,1)S(1)} %get-tuple-element.29), channel_id=1, source_target_pairs={{0,1},{1,0},{2,3},{3,2},{4,5},{5,4},{6,7},{7,6},{8,9},{9,8},{10,11... | collective-permute-start | bytes 393224 | tf_op jit(solution)/shard_map/ppermute | solution.py:50
  95.0 11.1 %collective-permute-start.37 = (bf16[64,2048]{1,0:T(8,128)(2,1)S(1)}, bf16[64,2048]{1,0:T(8,128)(2,1)S(1)}, u32[]{:S(2)}, u32[]{:S(2)}) collective-permute-start(bf16[64,2048]{1,0:T(8,128)(2,1)S(1)} %shard_map.152), channel_id=1, source_target_pairs={{0,24},{1,29},{2,26},{3,31},{4,28},{5,25},{6,30},{7,27},{8,16},{9,... | collective-permute-start | bytes 786440 | tf_op jit(solution)/shard_map/ppermute | solution.py:342
  95.3 25.4 %collective-permute-start.29 = (bf16[64,2048]{1,0:T(8,128)(2,1)S(1)}, bf16[64,2048]{1,0:T(8,128)(2,1)S(1)}, u32[]{:S(2)}, u32[]{:S(2)}) collective-permute-start(bf16[64,2048]{1,0:T(8,128)(2,1)S(1)} %shard_map.150), channel_id=1, source_target_pairs={{0,16},{1,21},{2,18},{3,23},{4,20},{5,17},{6,22},{7,19},{8,24},{9,... | collective-permute-start | bytes 786440 | tf_op jit(solution)/shard_map/ppermute | solution.py:342
  99.0 22.3 %collective-permute-start.21 = (bf16[64,2048]{1,0:T(8,128)(2,1)S(1)}, bf16[64,2048]{1,0:T(8,128)(2,1)S(1)}, u32[]{:S(2)}, u32[]{:S(2)}) collective-permute-start(bf16[64,2048]{1,0:T(8,128)(2,1)S(1)} %shard_map.148), channel_id=1, source_target_pairs={{0,8},{1,13},{2,10},{3,15},{4,12},{5,9},{6,14},{7,11},{8,0},{9,5},... | collective-permute-start | bytes 786440 | tf_op jit(solution)/shard_map/ppermute | solution.py:342
  100.5 21.6 %collective-permute-start.3 = (bf16[256,256]{1,0:T(8,128)(2,1)S(1)}, bf16[256,256]{1,0:T(8,128)(2,1)S(1)}, u32[]{:S(2)}, u32[]{:S(2)}) collective-permute-start(bf16[256,256]{1,0:T(8,128)(2,1)S(1)} %get-tuple-element.31), channel_id=1, source_target_pairs={{0,3},{1,2},{2,1},{3,0},{4,7},{5,6},{6,5},{7,4},{8,11},{9,10},{10,... | collective-permute-start | bytes 393224 | tf_op jit(solution)/shard_map/ppermute | solution.py:50
  100.5 24.9 %collective-permute-start.38 = (bf16[64,2048]{1,0:T(8,128)(2,1)S(1)}, bf16[64,2048]{1,0:T(8,128)(2,1)S(1)}, u32[]{:S(2)}, u32[]{:S(2)}) collective-permute-start(bf16[64,2048]{1,0:T(8,128)(2,1)S(1)} %broadcast_select_fusion.1.refs_0_), channel_id=1, source_target_pairs={{0,1},{1,0},{2,3},{3,2},{4,5},{5,4},{6,7},{7,6},{8,9},{9,8},{10,11... | collective-permute-start | bytes 786440 | tf_op jit(solution)/shard_map/ppermute | solution.py:50
  106.0 19.4 %collective-permute-start.41 = (bf16[64,2048]{1,0:T(8,128)(2,1)S(1)}, bf16[64,2048]{1,0:T(8,128)(2,1)S(1)}, u32[]{:S(2)}, u32[]{:S(2)}) collective-permute-start(bf16[64,2048]{1,0:T(8,128)(2,1)S(1)} %collective-permute-done.37.refs_3_), channel_id=1, source_target_pairs={{0,1},{1,0},{2,3},{3,2},{4,5},{5,4},{6,7},{7,6},{8,9},{9,8},{10,11... | collective-permute-start | bytes 786440 | tf_op jit(solution)/shard_map/ppermute | solution.py:50
  (33 other events, 284.1 us)

commit v3 on v2

--- a/solution.py
+++ b/solution.py
@@ -33,12 +33,12 @@
     return lax.broadcasted_iota(jnp.int32, shape, dim)
 
 
-def call(body, outs, specs, args, scratch, flops, vmem):
+def call(body, outs, specs, args, scratch, flops, vmem, place=VMEM):
     return pl.pallas_call(
         body,
         out_shape=outs,
         in_specs=specs,
-        out_specs=jax.tree.map(lambda _: VMEM, outs),
+        out_specs=jax.tree.map(lambda _: place, outs),
         scratch_shapes=scratch,
         cost_estimate=pl.CostEstimate(flops=flops, bytes_accessed=1 << 20, transcendentals=0),
         compiler_params=pltpu.CompilerParams(vmem_limit_bytes=vmem << 20),
@@ -215,15 +215,21 @@
 
 
 def final_body(pos, *refs):
-    sources, out = refs[:-1], refs[-1]
+    sources, out, built, sems = refs[:-3], refs[-3], refs[-2], refs[-1]
     depth = sum(r.shape[0] for r in sources)
     tokens, width = out.shape
     pick = (iota((tokens, depth), 1) == pos[:, 0:1].astype(jnp.int32)).astype(BF16)
     block = 512
+    copies = []
     for c in range(width // block):
         cols = slice(c * block, (c + 1) * block)
         value = jnp.concatenate([r[:, cols] for r in sources], axis=0)
-        out[:, cols] = dot(pick, value).astype(BF16)
+        built[:, cols] = dot(pick, value).astype(BF16)
+        at = pl.ds(c * block, block)
+        copies.append(pltpu.make_async_copy(built.at[:, at], out.at[:, at], sems.at[c]))
+        copies[-1].start()
+    for copy in copies:
+        copy.wait()
 
 
 def conv_body(reach, where, edge, *refs):
@@ -274,7 +280,7 @@
         out[:, cols] = total.astype(BF16)
         return carry
 
-    lax.fori_loop(0, width // block, columns, 0)
+    lax.fori_loop(0, width // block, columns, 0, unroll=True)
 
 
 def shards(
@@ -422,9 +428,10 @@
         jax.ShapeDtypeStruct((tokens, width), BF16),
         [VMEM] * (1 + 2 * n_chunks),
         (back_pos, *ordered, *[swap(value, "tp", 1) for value in ordered]),
-        [],
+        [pltpu.VMEM((tokens, width), BF16), pltpu.SemaphoreType.DMA((width // 512,))],
         4 * tokens * tokens * width,
         8,
+        HBM,
     )
     return (mixed, moe_out)
 

time: 128 us -> 127 us (level)
  transfers between devices with their start and end apart: 42 -> 42, of which waited for: 7 -> 7; matrix products, arithmetic and copies ran while one was open for 1% -> 1% of each run, Pallas kernels for 18% -> 17%
where the time goes in v3:
time: 127 us
  waiting for transfers between devices  50.6 us (40%)
  starting transfers between devices  39.7 us (31%)
  Pallas kernels  25.3 us (20%)
  local copies, waits for them, and re-layouts  8.53 us (7%)
  other arithmetic  1.51 us (1%)
    ppermute x8, waiting for transfers between devices, across(): got = lax.ppermute(value, ('ep', 'tp'), pairs)  41 us
    ppermute x33, starting transfers between devices, swap(): return lax.ppermute(value, axis, [(i, i ^ mask) for i in range(count)])  25.3 us
    pallas_call x14, Pallas kernels, call(): pl.pallas_call(body, out_shape=outs, in_specs=specs, out_specs=jax.tree.m...  25.3 us
    ppermute x8, starting transfers between devices, across(): got = lax.ppermute(value, ('ep', 'tp'), pairs)  11.8 us
    ppermute x33, waiting for transfers between devices, swap(): return lax.ppermute(value, axis, [(i, i ^ mask) for i in range(count)])  9.61 us
    unnamed x26, local copies, waits for them, and re-layouts  8.52 us
    ppermute x1, starting transfers between devices, shards(): edge = lax.ppermute(edge, 'ep', [(i, i + 1) for i in range(groups - 1)])  2.62 us
  transfers between devices with their start and end apart: 42, of which 7 were waited for; matrix products, arithmetic and copies ran while one was open for 1% of the time, Pallas kernels for 17%

profile of v3, /device:TPU:0, one launch (start us, length us, event | category | flops | bytes accessed | tf_op | source)
XLA Modules:
  0.0 126.8 jit_solution(18252988730728187630)
XLA Ops:
  5.9 1.8 %shard_map.144 = (bf16[64,2176]{1,0:T(8,128)(2,1)S(1)}, bf16[64,2176]{1,0:T(8,128)(2,1)S(1)}, bf16[64,2176]{1,0:T(8,128)(2,1)S(1)}, bf16[64,2176]{1,0:T(8,128)(2,1)S(1)}) custom-call(s32[3]{0:T(128)S(1)} %pad_add_fusion.where, bf16[256,2176]{1,0:T(8,128)(2,1)S(1)} %get-tuple-element.32.own, s32[8,256]{1,0:T(8,128)S(1)} %get-tuple-element.33.place_own, ...), custom_call_target="tpu_custom_call" | custom-call | flops 21474836480 | bytes 1048576 | tf_op jit(solution)/shard_map/pallas_call | solution.py:37
  7.7 5.1 %collective-permute-start.30 = (bf16[64,2176]{1,0:T(8,128)(2,1)S(1)}, bf16[64,2176]{1,0:T(8,128)(2,1)S(1)}, u32[]{:S(2)}, u32[]{:S(2)}) collective-permute-start(bf16[64,2176]{1,0:T(8,128)(2,1)S(1)} %get-tuple-element.49), channel_id=1, source_target_pairs={{0,24},{1,29},{2,26},{3,31},{4,28},{5,25},{6,30},{7,27},{8,16},{9,... | collective-permute-start | bytes 835592 | tf_op jit(solution)/shard_map/ppermute | solution.py:348
  14.2 6.2 %collective-permute-done.30.refs_0_ = bf16[64,2176]{1,0:T(8,128)(2,1)S(1)} collective-permute-done((bf16[64,2176]{1,0:T(8,128)(2,1)S(1)}, bf16[64,2176]{1,0:T(8,128)(2,1)S(1)}, u32[]{:S(2)}, u32[]{:S(2)}) %collective-permute-start.30) | collective-permute-done | bytes 278560 | tf_op jit(solution)/shard_map/ppermute | solution.py:348
  20.4 1.9 %collective-permute-start.32 = (bf16[64,2176]{1,0:T(8,128)(2,1)S(1)}, bf16[64,2176]{1,0:T(8,128)(2,1)S(1)}, u32[]{:S(2)}, u32[]{:S(2)}) collective-permute-start(bf16[64,2176]{1,0:T(8,128)(2,1)S(1)} %collective-permute-done.30.refs_0_), channel_id=1, source_target_pairs={{0,2},{1,3},{2,0},{3,1},{4,6},{5,7},{6,4},{7,5},{8,10},{9,11},{10,... | collective-permute-start | bytes 835592 | tf_op jit(solution)/shard_map/ppermute | solution.py:50
  22.5 15.2 %collective-permute-done.22.refs_0_ = bf16[64,2176]{1,0:T(8,128)(2,1)S(1)} collective-permute-done((bf16[64,2176]{1,0:T(8,128)(2,1)S(1)}, bf16[64,2176]{1,0:T(8,128)(2,1)S(1)}, u32[]{:S(2)}, u32[]{:S(2)}) %collective-permute-start.22) | collective-permute-done | bytes 278560 | tf_op jit(solution)/shard_map/ppermute | solution.py:348
  40.3 6.9 %collective-permute-done.24.refs_2_ = bf16[64,2176]{1,0:T(8,128)(2,1)S(1)} collective-permute-done((bf16[64,2176]{1,0:T(8,128)(2,1)S(1)}, bf16[64,2176]{1,0:T(8,128)(2,1)S(1)}, u32[]{:S(2)}, u32[]{:S(2)}) %collective-permute-start.24) | collective-permute-done | bytes 278560 | tf_op jit(solution)/shard_map/ppermute | solution.py:50
  47.7 2.2 %copy-done = bf16[1,2048,1024]{2,1,0:T(8,128)(2,1)S(1)} copy-done((bf16[1,2048,1024]{2,1,0:T(8,128)(2,1)S(1)}, bf16[1,2048,1024]{2,1,0:T(8,128)(2,1)}, u32[]{:S(2)}) %copy-start) | copy-done | bytes 4194328
  49.9 2.2 %copy-done.2 = bf16[1,2048,1024]{2,1,0:T(8,128)(2,1)S(1)} copy-done((bf16[1,2048,1024]{2,1,0:T(8,128)(2,1)S(1)}, bf16[1,2048,1024]{2,1,0:T(8,128)(2,1)}, u32[]{:S(2)}) %copy-start.2) | copy-done | bytes 4194328
  52.1 2.2 %copy-done.3 = bf16[1,1024,2048]{2,1,0:T(8,128)(2,1)S(1)} copy-done((bf16[1,1024,2048]{2,1,0:T(8,128)(2,1)S(1)}, bf16[1,1024,2048]{2,1,0:T(8,128)(2,1)}, u32[]{:S(2)}) %copy-start.3) | copy-done | bytes 4194328
  54.3 2.7 %shard_map.151 = (bf16[32,2048]{1,0:T(8,128)(2,1)S(1)}, bf16[32,2048]{1,0:T(8,128)(2,1)S(1)}, bf16[32,2048]{1,0:T(8,128)(2,1)S(1)}, bf16[32,2048]{1,0:T(8,128)(2,1)S(1)}) custom-call(s32[3]{0:T(128)S(1)} %pad_add_fusion.where, bf16[64,2176]{1,0:T(8,128)(2,1)S(1)} %collective-permute-done.30.refs_0_, bf16[64,2176]{1,0:T(8,128)(2,1)S(1)} %collective-permute-done.31.refs_1_, ...), custom_call_target="tpu_custom_call" | custom-call | flops 1610612736 | bytes 1048576 | tf_op jit(solution)/shard_map/pallas_call | solution.py:37
  57.0 2.6 %collective-permute-start = (bf16[16,256]{1,0:T(8,128)(2,1)S(1)}, bf16[16,256]{1,0:T(8,128)(2,1)S(1)}, u32[]{:S(2)}, u32[]{:S(2)}) collective-permute-start(bf16[16,256]{1,0:T(8,128)(2,1)S(1)} %pad_maximum_fusion), channel_id=1, source_target_pairs={{0,4},{4,8},{8,12},{12,16},{16,20},{20,24},{24,28},{1,5},{5,9},{9,... | collective-permute-start | bytes 24584 | tf_op jit(solution)/shard_map/ppermute | solution.py:339
  60.3 2.7 %shard_map.145 = (bf16[32,2048]{1,0:T(8,128)(2,1)S(1)}, bf16[32,2048]{1,0:T(8,128)(2,1)S(1)}, bf16[32,2048]{1,0:T(8,128)(2,1)S(1)}, bf16[32,2048]{1,0:T(8,128)(2,1)S(1)}) custom-call(s32[3]{0:T(128)S(1)} %pad_add_fusion.where, bf16[64,2176]{1,0:T(8,128)(2,1)S(1)} %broadcast_select_fusion.refs_0_, bf16[64,2176]{1,0:T(8,128)(2,1)S(1)} %collective-permute-done.7.refs_1_, ...), custom_call_target="tpu_custom_call" | custom-call | flops 1610612736 | bytes 1048576 | tf_op jit(solution)/shard_map/pallas_call | solution.py:37
  63.2 1.5 %collective-permute-start.11 = (bf16[32,2048]{1,0:T(8,128)(2,1)S(1)}, bf16[32,2048]{1,0:T(8,128)(2,1)S(1)}, u32[]{:S(2)}, u32[]{:S(2)}) collective-permute-start(bf16[32,2048]{1,0:T(8,128)(2,1)S(1)} %get-tuple-element.37), channel_id=1, source_target_pairs={{0,2},{1,3},{2,0},{3,1},{4,6},{5,7},{6,4},{7,5},{8,10},{9,11},{10,... | collective-permute-start | bytes 393224 | tf_op jit(solution)/shard_map/ppermute | solution.py:50
  64.9 2.7 %shard_map.149 = (bf16[32,2048]{1,0:T(8,128)(2,1)S(1)}, bf16[32,2048]{1,0:T(8,128)(2,1)S(1)}, bf16[32,2048]{1,0:T(8,128)(2,1)S(1)}, bf16[32,2048]{1,0:T(8,128)(2,1)S(1)}) custom-call(s32[3]{0:T(128)S(1)} %pad_add_fusion.where, bf16[64,2176]{1,0:T(8,128)(2,1)S(1)} %collective-permute-done.22.refs_0_, bf16[64,2176]{1,0:T(8,128)(2,1)S(1)} %collective-permute-done.23.refs_1_, ...), custom_call_target="tpu_custom_call" | custom-call | flops 1610612736 | bytes 1048576 | tf_op jit(solution)/shard_map/pallas_call | solution.py:37
  72.9 2.7 %shard_map.147 = (bf16[32,2048]{1,0:T(8,128)(2,1)S(1)}, bf16[32,2048]{1,0:T(8,128)(2,1)S(1)}, bf16[32,2048]{1,0:T(8,128)(2,1)S(1)}, bf16[32,2048]{1,0:T(8,128)(2,1)S(1)}) custom-call(s32[3]{0:T(128)S(1)} %pad_add_fusion.where, bf16[64,2176]{1,0:T(8,128)(2,1)S(1)} %collective-permute-done.14.refs_0_, bf16[64,2176]{1,0:T(8,128)(2,1)S(1)} %collective-permute-done.15.refs_1_, ...), custom_call_target="tpu_custom_call" | custom-call | flops 1610612736 | bytes 1048576 | tf_op jit(solution)/shard_map/pallas_call | solution.py:37
  77.4 1.6 %collective-permute-start.19 = (bf16[32,2048]{1,0:T(8,128)(2,1)S(1)}, bf16[32,2048]{1,0:T(8,128)(2,1)S(1)}, u32[]{:S(2)}, u32[]{:S(2)}) collective-permute-start(bf16[32,2048]{1,0:T(8,128)(2,1)S(1)} %get-tuple-element.42), channel_id=1, source_target_pairs={{0,2},{1,3},{2,0},{3,1},{4,6},{5,7},{6,4},{7,5},{8,10},{9,11},{10,... | collective-permute-start | bytes 393224 | tf_op jit(solution)/shard_map/ppermute | solution.py:50
  79.2 1.5 %collective-permute-done.27.refs_3_ = bf16[32,2048]{1,0:T(8,128)(2,1)S(1)} collective-permute-done((bf16[32,2048]{1,0:T(8,128)(2,1)S(1)}, bf16[32,2048]{1,0:T(8,128)(2,1)S(1)}, u32[]{:S(2)}, u32[]{:S(2)}) %collective-permute-start.27) | collective-permute-done | bytes 131104 | tf_op jit(solution)/shard_map/ppermute | solution.py:50
  81.7 2.4 %shard_map.140 = (bf16[256,256]{1,0:T(8,128)(2,1)S(1)}, bf16[256,256]{1,0:T(8,128)(2,1)S(1)}, bf16[256,256]{1,0:T(8,128)(2,1)S(1)}, bf16[256,256]{1,0:T(8,128)(2,1)S(1)}) custom-call(s32[3]{0:T(128)S(1)} %pad_add_fusion.where, bf16[16,256]{1,0:T(8,128)(2,1)S(1)} %collective-permute-done.edge, bf16[1024,256]{1,0:T(8,128)(2,1)S(1)} %copy-done.6, ...), custom_call_target="tpu_custom_call" | custom-call | flops 21474836480 | bytes 1048576 | tf_op jit(solution)/shard_map/pallas_call | solution.py:37
  85.1 7.5 %collective-permute-start.1 = (bf16[256,256]{1,0:T(8,128)(2,1)S(1)}, bf16[256,256]{1,0:T(8,128)(2,1)S(1)}, u32[]{:S(2)}, u32[]{:S(2)}) collective-permute-start(bf16[256,256]{1,0:T(8,128)(2,1)S(1)} %get-tuple-element.29), channel_id=1, source_target_pairs={{0,1},{1,0},{2,3},{3,2},{4,5},{5,4},{6,7},{7,6},{8,9},{9,8},{10,11... | collective-permute-start | bytes 393224 | tf_op jit(solution)/shard_map/ppermute | solution.py:50
  93.6 1.6 %collective-permute-start.2 = (bf16[256,256]{1,0:T(8,128)(2,1)S(1)}, bf16[256,256]{1,0:T(8,128)(2,1)S(1)}, u32[]{:S(2)}, u32[]{:S(2)}) collective-permute-start(bf16[256,256]{1,0:T(8,128)(2,1)S(1)} %get-tuple-element.30), channel_id=1, source_target_pairs={{0,2},{1,3},{2,0},{3,1},{4,6},{5,7},{6,4},{7,5},{8,10},{9,11},{10,... | collective-permute-start | bytes 393224 | tf_op jit(solution)/shard_map/ppermute | solution.py:50
  95.5 2.7 %collective-permute-start.29 = (bf16[64,2048]{1,0:T(8,128)(2,1)S(1)}, bf16[64,2048]{1,0:T(8,128)(2,1)S(1)}, u32[]{:S(2)}, u32[]{:S(2)}) collective-permute-start(bf16[64,2048]{1,0:T(8,128)(2,1)S(1)} %shard_map.150), channel_id=1, source_target_pairs={{0,16},{1,21},{2,18},{3,23},{4,20},{5,17},{6,22},{7,19},{8,24},{9,... | collective-permute-start | bytes 786440 | tf_op jit(solution)/shard_map/ppermute | solution.py:348
  101.4 4.9 %collective-permute-done.37.refs_3_ = bf16[64,2048]{1,0:T(8,128)(2,1)S(1)} collective-permute-done((bf16[64,2048]{1,0:T(8,128)(2,1)S(1)}, bf16[64,2048]{1,0:T(8,128)(2,1)S(1)}, u32[]{:S(2)}, u32[]{:S(2)}) %collective-permute-start.37) | collective-permute-done | bytes 262176 | tf_op jit(solution)/shard_map/ppermute | solution.py:348
  106.3 14.7 %collective-permute-done.29.refs_2_ = bf16[64,2048]{1,0:T(8,128)(2,1)S(1)} collective-permute-done((bf16[64,2048]{1,0:T(8,128)(2,1)S(1)}, bf16[64,2048]{1,0:T(8,128)(2,1)S(1)}, u32[]{:S(2)}, u32[]{:S(2)}) %collective-permute-start.29) | collective-permute-done | bytes 262176 | tf_op jit(solution)/shard_map/ppermute | solution.py:348
  122.3 2.8 %shard_map.141 = bf16[256,2048]{1,0:T(8,128)(2,1)} custom-call(s32[3]{0:T(128)S(1)} %pad_add_fusion.where, bf16[1024,2048]{1,0:T(8,128)(2,1)S(1)} %copy-done.4, bf16[256,256]{1,0:T(8,128)(2,1)S(1)} %get-tuple-element.28.refs_0_, bf16[256,256]{1,0:T(8,128)(2,1)S(1)} %collective-permute-done.1.refs_1_, bf16[256,256]{1,0:T(8,128)(2,1)S(1)} %collective-permute-done.2.refs_2_, ...), custom_call_target="tpu_custom_call" | custom-call | flops 1073741824 | bytes 1048576 | tf_op jit(solution)/shard_map/pallas_call | solution.py:37
  (110 shorter events, 27.2 us)
Async XLA Ops:
  7.7 12.7 %collective-permute-start.30 = (bf16[64,2176]{1,0:T(8,128)(2,1)S(1)}, bf16[64,2176]{1,0:T(8,128)(2,1)S(1)}, u32[]{:S(2)}, u32[]{:S(2)}) collective-permute-start(bf16[64,2176]{1,0:T(8,128)(2,1)S(1)} %get-tuple-element.49), channel_id=1, source_target_pairs={{0,24},{1,29},{2,26},{3,31},{4,28},{5,25},{6,30},{7,27},{8,16},{9,... | collective-permute-start | bytes 835592 | tf_op jit(solution)/shard_map/ppermute | solution.py:348
  12.9 9.4 %collective-permute-start.6 = (bf16[64,2176]{1,0:T(8,128)(2,1)S(1)}, bf16[64,2176]{1,0:T(8,128)(2,1)S(1)}, u32[]{:S(2)}, u32[]{:S(2)}) collective-permute-start(bf16[64,2176]{1,0:T(8,128)(2,1)S(1)} %get-tuple-element.34), channel_id=1, source_target_pairs={{1,5},{3,7},{5,1},{7,3},{9,13},{11,15},{13,9},{15,11},{17,21},{19,... | collective-permute-start | bytes 835592 | tf_op jit(solution)/shard_map/ppermute | solution.py:348
  13.5 24.1 %collective-permute-start.22 = (bf16[64,2176]{1,0:T(8,128)(2,1)S(1)}, bf16[64,2176]{1,0:T(8,128)(2,1)S(1)}, u32[]{:S(2)}, u32[]{:S(2)}) collective-permute-start(bf16[64,2176]{1,0:T(8,128)(2,1)S(1)} %get-tuple-element.44), channel_id=1, source_target_pairs={{0,16},{1,21},{2,18},{3,23},{4,20},{5,17},{6,22},{7,19},{8,24},{9,... | collective-permute-start | bytes 835592 | tf_op jit(solution)/shard_map/ppermute | solution.py:348
  13.6 25.6 %collective-permute-start.14 = (bf16[64,2176]{1,0:T(8,128)(2,1)S(1)}, bf16[64,2176]{1,0:T(8,128)(2,1)S(1)}, u32[]{:S(2)}, u32[]{:S(2)}) collective-permute-start(bf16[64,2176]{1,0:T(8,128)(2,1)S(1)} %get-tuple-element.39), channel_id=1, source_target_pairs={{0,8},{1,13},{2,10},{3,15},{4,12},{5,9},{6,14},{7,11},{8,0},{9,5},... | collective-permute-start | bytes 835592 | tf_op jit(solution)/shard_map/ppermute | solution.py:348
  20.4 18.8 %collective-permute-start.32 = (bf16[64,2176]{1,0:T(8,128)(2,1)S(1)}, bf16[64,2176]{1,0:T(8,128)(2,1)S(1)}, u32[]{:S(2)}, u32[]{:S(2)}) collective-permute-start(bf16[64,2176]{1,0:T(8,128)(2,1)S(1)} %collective-permute-done.30.refs_0_), channel_id=1, source_target_pairs={{0,2},{1,3},{2,0},{3,1},{4,6},{5,7},{6,4},{7,5},{8,10},{9,11},{10,... | collective-permute-start | bytes 835592 | tf_op jit(solution)/shard_map/ppermute | solution.py:50
  22.3 17.5 %collective-permute-start.31 = (bf16[64,2176]{1,0:T(8,128)(2,1)S(1)}, bf16[64,2176]{1,0:T(8,128)(2,1)S(1)}, u32[]{:S(2)}, u32[]{:S(2)}) collective-permute-start(bf16[64,2176]{1,0:T(8,128)(2,1)S(1)} %collective-permute-done.30.refs_0_), channel_id=1, source_target_pairs={{0,1},{1,0},{2,3},{3,2},{4,5},{5,4},{6,7},{7,6},{8,9},{9,8},{10,11... | collective-permute-start | bytes 835592 | tf_op jit(solution)/shard_map/ppermute | solution.py:50
  22.3 17.6 %collective-permute-start.8 = (bf16[64,2176]{1,0:T(8,128)(2,1)S(1)}, bf16[64,2176]{1,0:T(8,128)(2,1)S(1)}, u32[]{:S(2)}, u32[]{:S(2)}) collective-permute-start(bf16[64,2176]{1,0:T(8,128)(2,1)S(1)} %broadcast_select_fusion.refs_0_), channel_id=1, source_target_pairs={{0,2},{1,3},{2,0},{3,1},{4,6},{5,7},{6,4},{7,5},{8,10},{9,11},{10,... | collective-permute-start | bytes 835592 | tf_op jit(solution)/shard_map/ppermute | solution.py:50
  37.7 9.5 %collective-permute-start.24 = (bf16[64,2176]{1,0:T(8,128)(2,1)S(1)}, bf16[64,2176]{1,0:T(8,128)(2,1)S(1)}, u32[]{:S(2)}, u32[]{:S(2)}) collective-permute-start(bf16[64,2176]{1,0:T(8,128)(2,1)S(1)} %collective-permute-done.22.refs_0_), channel_id=1, source_target_pairs={{0,2},{1,3},{2,0},{3,1},{4,6},{5,7},{6,4},{7,5},{8,10},{9,11},{10,... | collective-permute-start | bytes 835592 | tf_op jit(solution)/shard_map/ppermute | solution.py:50
  39.2 17.8 %collective-permute-start.16 = (bf16[64,2176]{1,0:T(8,128)(2,1)S(1)}, bf16[64,2176]{1,0:T(8,128)(2,1)S(1)}, u32[]{:S(2)}, u32[]{:S(2)}) collective-permute-start(bf16[64,2176]{1,0:T(8,128)(2,1)S(1)} %collective-permute-done.14.refs_0_), channel_id=1, source_target_pairs={{0,2},{1,3},{2,0},{3,1},{4,6},{5,7},{6,4},{7,5},{8,10},{9,11},{10,... | collective-permute-start | bytes 835592 | tf_op jit(solution)/shard_map/ppermute | solution.py:50
  39.8 19.9 %collective-permute-start.7 = (bf16[64,2176]{1,0:T(8,128)(2,1)S(1)}, bf16[64,2176]{1,0:T(8,128)(2,1)S(1)}, u32[]{:S(2)}, u32[]{:S(2)}) collective-permute-start(bf16[64,2176]{1,0:T(8,128)(2,1)S(1)} %broadcast_select_fusion.refs_0_), channel_id=1, source_target_pairs={{0,1},{1,0},{2,3},{3,2},{4,5},{5,4},{6,7},{7,6},{8,9},{9,8},{10,11... | collective-permute-start | bytes 835592 | tf_op jit(solution)/shard_map/ppermute | solution.py:50
  40.0 19.8 %collective-permute-start.9 = (bf16[64,2176]{1,0:T(8,128)(2,1)S(1)}, bf16[64,2176]{1,0:T(8,128)(2,1)S(1)}, u32[]{:S(2)}, u32[]{:S(2)}) collective-permute-start(bf16[64,2176]{1,0:T(8,128)(2,1)S(1)} %collective-permute-done.8.refs_2_), channel_id=1, source_target_pairs={{0,1},{1,0},{2,3},{3,2},{4,5},{5,4},{6,7},{7,6},{8,9},{9,8},{10,11... | collective-permute-start | bytes 835592 | tf_op jit(solution)/shard_map/ppermute | solution.py:50
  47.2 15.9 %collective-permute-start.23 = (bf16[64,2176]{1,0:T(8,128)(2,1)S(1)}, bf16[64,2176]{1,0:T(8,128)(2,1)S(1)}, u32[]{:S(2)}, u32[]{:S(2)}) collective-permute-start(bf16[64,2176]{1,0:T(8,128)(2,1)S(1)} %collective-permute-done.22.refs_0_), channel_id=1, source_target_pairs={{0,1},{1,0},{2,3},{3,2},{4,5},{5,4},{6,7},{7,6},{8,9},{9,8},{10,11... | collective-permute-start | bytes 835592 | tf_op jit(solution)/shard_map/ppermute | solution.py:50
  47.2 17.5 %collective-permute-start.25 = (bf16[64,2176]{1,0:T(8,128)(2,1)S(1)}, bf16[64,2176]{1,0:T(8,128)(2,1)S(1)}, u32[]{:S(2)}, u32[]{:S(2)}) collective-permute-start(bf16[64,2176]{1,0:T(8,128)(2,1)S(1)} %collective-permute-done.24.refs_2_), channel_id=1, source_target_pairs={{0,1},{1,0},{2,3},{3,2},{4,5},{5,4},{6,7},{7,6},{8,9},{9,8},{10,11... | collective-permute-start | bytes 835592 | tf_op jit(solution)/shard_map/ppermute | solution.py:50
  77.4 16.2 %collective-permute-start.18 = (bf16[32,2048]{1,0:T(8,128)(2,1)S(1)}, bf16[32,2048]{1,0:T(8,128)(2,1)S(1)}, u32[]{:S(2)}, u32[]{:S(2)}) collective-permute-start(bf16[32,2048]{1,0:T(8,128)(2,1)S(1)} %get-tuple-element.41), channel_id=1, source_target_pairs={{0,1},{1,0},{2,3},{3,2},{4,5},{5,4},{6,7},{7,6},{8,9},{9,8},{10,11... | collective-permute-start | bytes 393224 | tf_op jit(solution)/shard_map/ppermute | solution.py:50
  77.4 17.8 %collective-permute-start.19 = (bf16[32,2048]{1,0:T(8,128)(2,1)S(1)}, bf16[32,2048]{1,0:T(8,128)(2,1)S(1)}, u32[]{:S(2)}, u32[]{:S(2)}) collective-permute-start(bf16[32,2048]{1,0:T(8,128)(2,1)S(1)} %get-tuple-element.42), channel_id=1, source_target_pairs={{0,2},{1,3},{2,0},{3,1},{4,6},{5,7},{6,4},{7,5},{8,10},{9,11},{10,... | collective-permute-start | bytes 393224 | tf_op jit(solution)/shard_map/ppermute | solution.py:50
  79.0 16.5 %collective-permute-start.20 = (bf16[32,2048]{1,0:T(8,128)(2,1)S(1)}, bf16[32,2048]{1,0:T(8,128)(2,1)S(1)}, u32[]{:S(2)}, u32[]{:S(2)}) collective-permute-start(bf16[32,2048]{1,0:T(8,128)(2,1)S(1)} %get-tuple-element.43), channel_id=1, source_target_pairs={{0,3},{1,2},{2,1},{3,0},{4,7},{5,6},{6,5},{7,4},{8,11},{9,10},{10,... | collective-permute-start | bytes 393224 | tf_op jit(solution)/shard_map/ppermute | solution.py:50
  80.8 18.4 %collective-permute-start.13 = (bf16[64,2048]{1,0:T(8,128)(2,1)S(1)}, bf16[64,2048]{1,0:T(8,128)(2,1)S(1)}, u32[]{:S(2)}, u32[]{:S(2)}) collective-permute-start(bf16[64,2048]{1,0:T(8,128)(2,1)S(1)} %shard_map.146), channel_id=1, source_target_pairs={{1,5},{3,7},{5,1},{7,3},{9,13},{11,15},{13,9},{15,11},{17,21},{19,... | collective-permute-start | bytes 786440 | tf_op jit(solution)/shard_map/ppermute | solution.py:348
  85.1 15.6 %collective-permute-start.1 = (bf16[256,256]{1,0:T(8,128)(2,1)S(1)}, bf16[256,256]{1,0:T(8,128)(2,1)S(1)}, u32[]{:S(2)}, u32[]{:S(2)}) collective-permute-start(bf16[256,256]{1,0:T(8,128)(2,1)S(1)} %get-tuple-element.29), channel_id=1, source_target_pairs={{0,1},{1,0},{2,3},{3,2},{4,5},{5,4},{6,7},{7,6},{8,9},{9,8},{10,11... | collective-permute-start | bytes 393224 | tf_op jit(solution)/shard_map/ppermute | solution.py:50
  95.2 11.1 %collective-permute-start.37 = (bf16[64,2048]{1,0:T(8,128)(2,1)S(1)}, bf16[64,2048]{1,0:T(8,128)(2,1)S(1)}, u32[]{:S(2)}, u32[]{:S(2)}) collective-permute-start(bf16[64,2048]{1,0:T(8,128)(2,1)S(1)} %shard_map.152), channel_id=1, source_target_pairs={{0,24},{1,29},{2,26},{3,31},{4,28},{5,25},{6,30},{7,27},{8,16},{9,... | collective-permute-start | bytes 786440 | tf_op jit(solution)/shard_map/ppermute | solution.py:348
  95.5 25.4 %collective-permute-start.29 = (bf16[64,2048]{1,0:T(8,128)(2,1)S(1)}, bf16[64,2048]{1,0:T(8,128)(2,1)S(1)}, u32[]{:S(2)}, u32[]{:S(2)}) collective-permute-start(bf16[64,2048]{1,0:T(8,128)(2,1)S(1)} %shard_map.150), channel_id=1, source_target_pairs={{0,16},{1,21},{2,18},{3,23},{4,20},{5,17},{6,22},{7,19},{8,24},{9,... | collective-permute-start | bytes 786440 | tf_op jit(solution)/shard_map/ppermute | solution.py:348
  99.2 22.3 %collective-permute-start.21 = (bf16[64,2048]{1,0:T(8,128)(2,1)S(1)}, bf16[64,2048]{1,0:T(8,128)(2,1)S(1)}, u32[]{:S(2)}, u32[]{:S(2)}) collective-permute-start(bf16[64,2048]{1,0:T(8,128)(2,1)S(1)} %shard_map.148), channel_id=1, source_target_pairs={{0,8},{1,13},{2,10},{3,15},{4,12},{5,9},{6,14},{7,11},{8,0},{9,5},... | collective-permute-start | bytes 786440 | tf_op jit(solution)/shard_map/ppermute | solution.py:348
  100.7 21.7 %collective-permute-start.3 = (bf16[256,256]{1,0:T(8,128)(2,1)S(1)}, bf16[256,256]{1,0:T(8,128)(2,1)S(1)}, u32[]{:S(2)}, u32[]{:S(2)}) collective-permute-start(bf16[256,256]{1,0:T(8,128)(2,1)S(1)} %get-tuple-element.31), channel_id=1, source_target_pairs={{0,3},{1,2},{2,1},{3,0},{4,7},{5,6},{6,5},{7,4},{8,11},{9,10},{10,... | collective-permute-start | bytes 393224 | tf_op jit(solution)/shard_map/ppermute | solution.py:50
  100.8 24.4 %collective-permute-start.38 = (bf16[64,2048]{1,0:T(8,128)(2,1)S(1)}, bf16[64,2048]{1,0:T(8,128)(2,1)S(1)}, u32[]{:S(2)}, u32[]{:S(2)}) collective-permute-start(bf16[64,2048]{1,0:T(8,128)(2,1)S(1)} %broadcast_select_fusion.1.refs_0_), channel_id=1, source_target_pairs={{0,1},{1,0},{2,3},{3,2},{4,5},{5,4},{6,7},{7,6},{8,9},{9,8},{10,11... | collective-permute-start | bytes 786440 | tf_op jit(solution)/shard_map/ppermute | solution.py:50
  106.3 18.9 %collective-permute-start.41 = (bf16[64,2048]{1,0:T(8,128)(2,1)S(1)}, bf16[64,2048]{1,0:T(8,128)(2,1)S(1)}, u32[]{:S(2)}, u32[]{:S(2)}) collective-permute-start(bf16[64,2048]{1,0:T(8,128)(2,1)S(1)} %collective-permute-done.37.refs_3_), channel_id=1, source_target_pairs={{0,1},{1,0},{2,3},{3,2},{4,5},{5,4},{6,7},{7,6},{8,9},{9,8},{10,11... | collective-permute-start | bytes 786440 | tf_op jit(solution)/shard_map/ppermute | solution.py:50
  (33 other events, 284.5 us)
